TPU v7x, 32 devices: a whole 2x2x4 slice. The times are simulated.
32 devices in a mesh: grp: 2 (over y), fs: 4 (over z), tp: 4 (over x, core).
Axes of the slice: x: 2, y: 2, z: 4, core: 2. Of those that a mesh axis runs over, the one named last changes fastest.
Arguments:
- tokens: bfloat16 [32, 128, 2048], P(('grp', 'fs'), None, 'tp'), parts along dimension 0, may hold values from -100 to 100
- mix_gain: float32 [2048], replicated, may hold values from 0.1 to 1.9
- gate_outer: bfloat16 [2048, 1024], P('fs', 'tp'), may hold values from -0.125 to 0.125
- gate_inner: bfloat16 [2048, 1024], P('fs', 'tp'), may hold values from -0.125 to 0.125
- value_weight: bfloat16 [2048, 1024], P('fs', 'tp'), may hold values from -0.125 to 0.125
- conv_taps: float32 [3, 1024], replicated, may hold values from -3 to 3
- mix_out: bfloat16 [1024, 2048], P('tp', 'fs'), may hold values from -0.25 to 0.25
- ffn_gain: float32 [2048], replicated, may hold values from 0.1 to 1.9
- ffn_gate: bfloat16 [2048, 5632], P('fs', 'tp'), may hold values from -0.125 to 0.125
- ffn_up: bfloat16 [2048, 5632], P('fs', 'tp'), may hold values from -0.125 to 0.125
- ffn_down: bfloat16 [5632, 2048], P('tp', 'fs'), may hold values from -0.109375 to 0.109375
- out_gain: float32 [2048], replicated, may hold values from 0.1 to 1.9
Outputs:
- layer_out: bfloat16 [32, 128, 2048], P(('grp', 'fs'), None, 'tp'), parts along dimension 0
There are 2 independent parts, one for each index of `grp`. A program takes and returns all parts, laid end to end along the dimension named above; an argument that names none is the same for every part. Nothing has to cross between parts.
All inputs are finite; a program needn't handle non-finite values.
Results may differ from a plain program's by a relative error of at most 0.015.
Values may be sent and summed in bfloat16 or wider, within the bound.
A program may use at most 64 MiB of HBM per device.

v0:
```python
import functools

import jax
import jax.numpy as jnp
from jax import lax
from jax.experimental import pallas as pl
from jax.experimental.pallas import tpu as pltpu
from jax.sharding import PartitionSpec as P

MESH = pl.DeviceIdType.MESH
F32 = jnp.float32
BF16 = jnp.bfloat16
MIXER = 4
GATE, UP, DOWN = 4, 5, 6


def chunks_of(half):
    return next(count for count in (4, 2, 1) if half % (count * 16) == 0 or count == 1)


def column(rows):
    wide = jnp.broadcast_to(rows, (rows.shape[1], rows.shape[1]))
    return jnp.transpose(wide)[:, :1]


def kernel(
    n, parts, n_tp, length, chunk_counts,
    tok_ref, mix_gain, w0, w1, w2, taps_ref, w3, ffn_gain, w4, w5, w6, out_gain,
    out_ref,
    f0, f1, f2, f3, f4, f5, f6,
    tok_full, normed, proj, gated, part, pair_recv, far_recv, first_full, hidden, returned, sq_send, sq_recv,
    right_send, left_send, z_recv, y_send, y_recv, own_sem, pair_ss, pair_rs, far_ss, far_rs,
    down_pair_ss, down_pair_rs, down_far_ss, down_far_rs, sq_ss, sq_rs, guest_sem,
):
    own = (w0, w1, w2, w3, w4, w5, w6)
    full = (f0, f1, f2, f3, f4, f5, f6)
    f, g, t = lax.axis_index("fs"), lax.axis_index("grp"), lax.axis_index("tp")
    rows, columns = tok_ref.shape
    width = columns * n_tp
    seqs = rows // length
    bases = [sum(chunk_counts[:w]) for w in range(7)]

    def y_peer(k):
        return lax.rem(g + k, parts)

    def tp_peer(k):
        return lax.rem(t + k, n_tp)

    def span(w, half, c):
        size = own[w].shape[0] // parts
        piece = size // chunk_counts[w]
        start = half * size + c * piece
        return pl.ds(pl.multiple_of(start, 8), piece)

    def region(w, blk, half, c):
        return full[w].at[blk, span(w, half, c), :]

    barrier = pltpu.get_barrier_semaphore()
    for k in range(1, n_tp):
        pl.semaphore_signal(barrier, inc=1, device_id={"tp": tp_peer(k)}, device_id_type=MESH)
    for k in range(1, parts):
        pl.semaphore_signal(barrier, inc=1, device_id={"grp": y_peer(k)}, device_id_type=MESH)

    @pl.when(f < n - 1)
    def _():
        pl.semaphore_signal(barrier, inc=1, device_id={"fs": f + 1}, device_id_type=MESH)

    @pl.when(f > 0)
    def _():
        pl.semaphore_signal(barrier, inc=1, device_id={"fs": f - 1}, device_id_type=MESH)

    neighbours = lax.min(f, 1) + lax.min(n - 1 - f, 1)
    pl.semaphore_wait(barrier, n_tp - 1 + parts - 1 + neighbours)

    def z_copy(w, c, blk, src, step):
        send = right_send if step > 0 else left_send
        return pltpu.make_async_remote_copy(
            src_ref=src, dst_ref=region(w, blk, g, c),
            send_sem=send.at[bases[w] + c, blk], recv_sem=z_recv.at[bases[w] + c, blk],
            device_id={"fs": f + step}, device_id_type=MESH,
        )

    def y_copy(w, c, blk, half, k, peer):
        return pltpu.make_async_remote_copy(
            src_ref=region(w, blk, half, c), dst_ref=region(w, blk, half, c),
            send_sem=y_send.at[bases[w] + c, blk, k - 1], recv_sem=y_recv.at[bases[w] + c, blk, k - 1],
            device_id={"grp": peer}, device_id_type=MESH,
        )

    first_host, last_host = 1, n - 2
    is_host = (f >= first_host) & (f <= last_host)

    def start_own(w):
        @pl.loop(0, chunk_counts[w])
        def _(c):
            src = own[w].at[span(w, g, c), :]

            @pl.when(f + 1 <= last_host)
            def _():
                z_copy(w, c, f, src, 1).start()

            @pl.when(f - 1 >= first_host)
            def _():
                z_copy(w, c, f, src, -1).start()

    def other_half(w, c, k):
        half = lax.rem(g + parts - k, parts)
        inward = lax.select(f == 0, 1, n - 2)
        return pltpu.make_async_remote_copy(
            src_ref=own[w].at[span(w, half, c), :], dst_ref=region(w, f, half, c),
            send_sem=y_send.at[bases[w] + c, f, k - 1], recv_sem=y_recv.at[bases[w] + c, f, k - 1],
            device_id={"fs": inward}, device_id_type=MESH,
        )

    def receive(w, s):
        left, right = f - 1 - s, f + 1 + s

        @pl.loop(0, chunk_counts[w])
        def _(c):
            def arrived(blk, step, whole):
                z_copy(w, c, blk, region(w, blk, g, c), -step).wait_recv()
                onward = (f + 1 <= last_host) if step > 0 else (f - 1 >= first_host)

                @pl.when(onward)
                def _():
                    z_copy(w, c, blk, region(w, blk, g, c), step).start()

                def share():
                    for k in range(1, parts):
                        y_copy(w, c, blk, g, k, y_peer(k)).start()

                if s == 0:
                    pl.when(jnp.logical_not(whole))(share)
                else:
                    share()

            @pl.when(right < n)
            def _():
                arrived(right, -1, right == n - 1)

            @pl.when(left >= 0)
            def _():
                arrived(left, 1, left == 0)

    def finish(w, s):
        @pl.loop(0, chunk_counts[w])
        def _(c):
            for k in range(1, parts):
                source = lax.rem(g + parts - k, parts)
                for blk, there in ((f - 1 - s, f - 1 - s >= 0), (f + 1 + s, f + 1 + s < n)):
                    @pl.when(there)
                    def _():
                        y_copy(w, c, blk, source, k, source).wait_recv()

    def own_copy(w):
        return pltpu.make_async_copy(own[w], full[w].at[f], own_sem.at[w])

    def own_columns(owner):
        return pl.ds(pl.multiple_of(owner * columns, 128), columns)

    chips = n_tp // 2
    core = lax.rem(t, 2)
    pair = t + 1 - 2 * core

    def ahead(k, start=None):
        return lax.rem((t if start is None else start) + 2 * k, n_tp)

    def behind(k, start=None):
        return lax.rem((t if start is None else start) + n_tp - 2 * k, n_tp)

    def set_rows(r):
        return pl.ds(r * rows, rows)

    def pair_copy(stage, r, k, src, dst):
        return pltpu.make_async_remote_copy(
            src_ref=src, dst_ref=dst, send_sem=pair_ss.at[stage, r, k], recv_sem=pair_rs.at[stage, r, k],
            device_id={"tp": pair}, device_id_type=MESH,
        )

    def far_copy(stage, r, k, src, dst, peer):
        return pltpu.make_async_remote_copy(
            src_ref=src, dst_ref=dst, send_sem=far_ss.at[stage, r, k], recv_sem=far_rs.at[stage, r, k],
            device_id={"tp": peer}, device_id_type=MESH,
        )

    def block_of(buf, r, owner):
        return buf.at[set_rows(r), own_columns(owner)]

    def gather_send(buf, stage, r):
        mine = block_of(buf, r, t)
        for k in range(1, chips):
            far_copy(stage, r, k, mine, mine, ahead(k)).start()
        pair_copy(stage, r, 0, mine, mine).start()

    def gather_relay(buf, stage, r):
        for k in range(1, chips):
            theirs = block_of(buf, r, behind(k))
            far_copy(stage, r, k, theirs, theirs, behind(k)).wait_recv()
            pair_copy(stage, r, k, theirs, theirs).start()

    def gather_finish(buf, stage, r):
        for k in range(chips):
            theirs = block_of(buf, r, behind(k, pair))
            pair_copy(stage, r, k, theirs, theirs).wait_recv()

    def gather_sent(buf, stage, r):
        mine = block_of(buf, r, t)
        for k in range(1, chips):
            far_copy(stage, r, k, mine, mine, ahead(k)).wait_send()
        for k in range(chips):
            pair_copy(stage, r, k, mine, mine).wait_send()

    def to_pair(r, k):
        return pair_copy(1, r, k, block_of(part, r, ahead(k, pair)), pair_recv.at[r, k])

    def to_far(r, k):
        return far_copy(1, r, k, block_of(part, r, ahead(k)), far_recv.at[r, k], ahead(k))

    def sum_send(r):
        for k in range(chips - 1, -1, -1):
            to_pair(r, k).start()

    def sum_relay(r):
        for k in range(1, chips):
            to_pair(r, k).wait_recv()

            @pl.loop(0, rows // 64)
            def _(i):
                inside = pl.ds(pl.multiple_of(i * 64, 64), 64)
                at = pl.ds(pl.multiple_of(r * rows + i * 64, 64), 64)
                both = part[at, own_columns(ahead(k))].astype(F32) + pair_recv[r, k, inside, :].astype(F32)
                part[at, own_columns(ahead(k))] = both.astype(BF16)

            to_far(r, k).start()

    def summed(r, start, size):
        inside = pl.ds(pl.multiple_of(start, size), size)
        at = pl.ds(pl.multiple_of(r * rows + start, size), size)
        total = part[at, own_columns(t)].astype(F32) + pair_recv[r, 0, inside, :].astype(F32)
        for k in range(1, chips):
            total = total + far_recv[r, k, inside, :].astype(F32)
        return at, total

    def first_rows(r):
        to_pair(r, 0).wait_recv()
        for k in range(1, chips):
            to_far(r, k).wait_recv()

        @pl.loop(0, rows // 64)
        def _(i):
            at, total = summed(r, i * 64, 64)
            first_full[at, own_columns(t)] = (tok_full[at, own_columns(t)].astype(F32) + total).astype(BF16)

    def norm_rows(source, gain, r):
        size = 32

        @pl.loop(0, rows // size)
        def _(i):
            at = pl.ds(pl.multiple_of(r * rows + i * size, size), size)
            values = source[at, :].astype(F32)
            scale = lax.rsqrt(jnp.sum(values * values, axis=1, keepdims=True) / width + 1e-06)
            normed[at, :] = (values * scale * gain[...]).astype(BF16)

    channels = w0.shape[1]
    block = w3.shape[1]
    units = w4.shape[1]
    tap_count = taps_ref.shape[0]

    def mixer(r):
        for w in range(3):
            weight = full[w][...].reshape(width, channels)
            proj[w] = jnp.dot(normed[set_rows(r), :], weight, preferred_element_type=F32).astype(BF16)
        taps = taps_ref[:, pl.ds(pl.multiple_of(t * channels, 128), channels)]

        @pl.loop(0, seqs)
        def _(i):
            at = pl.ds(pl.multiple_of(i * length, length), length)
            product = proj[1, at, :].astype(F32) * proj[2, at, :].astype(F32)
            position = lax.broadcasted_iota(jnp.int32, product.shape, 0)
            conv = jnp.zeros_like(product)
            for offset in range(tap_count):
                shift = tap_count - 1 - offset
                moved = product if shift == 0 else jnp.where(position >= shift, pltpu.roll(product, shift, 0), 0.0)
                conv = conv + taps[offset : offset + 1, :] * moved
            gated[at, :] = (proj[0, at, :].astype(F32) * conv).astype(BF16)

        @pl.loop(0, n)
        def _(b):
            at = pl.ds(pl.multiple_of(b * block, 128), block)
            part[set_rows(r), at] = jnp.dot(gated[...], full[3][b], preferred_element_type=F32).astype(BF16)

    def hidden_tile(r, start, size):
        at = pl.ds(start, size)
        left = normed[set_rows(r), :]
        gate = jnp.dot(left, full[GATE][:, :, at].reshape(width, size), preferred_element_type=F32)
        upward = jnp.dot(left, full[UP][:, :, at].reshape(width, size), preferred_element_type=F32)
        hidden[set_rows(r), at] = (gate / (1.0 + jnp.exp(-gate)) * upward).astype(BF16)

    def hidden_rows(r):
        @pl.loop(0, units // 256)
        def _(j):
            hidden_tile(r, pl.multiple_of(j * 256, 256), 256)

        if units % 256:
            hidden_tile(r, units // 256 * 256, units % 256)

    wide = w6.shape[1]
    piece = min(wide, columns)
    per_block, per_owner = wide // piece, columns // piece

    def down_to_pair(r, k, slot, start):
        inside = pl.ds(pl.multiple_of(slot * piece, 128), piece)
        return pltpu.make_async_remote_copy(
            src_ref=part.at[set_rows(r), pl.ds(start, piece)], dst_ref=pair_recv.at[r, k, :, inside],
            send_sem=down_pair_ss.at[r, k, slot], recv_sem=down_pair_rs.at[r, k, slot],
            device_id={"tp": pair}, device_id_type=MESH,
        )

    def down_to_far(r, k, slot, start):
        inside = pl.ds(pl.multiple_of(slot * piece, 128), piece)
        return pltpu.make_async_remote_copy(
            src_ref=part.at[set_rows(r), pl.ds(start, piece)], dst_ref=far_recv.at[r, k, :, inside],
            send_sem=down_far_ss.at[r, k, slot], recv_sem=down_far_rs.at[r, k, slot],
            device_id={"tp": lax.rem(t + 2 * k, n_tp)}, device_id_type=MESH,
        )

    def down_block(b):
        for p in range(per_block):
            start = pl.multiple_of(b * wide + p * piece, 128)
            owner = (b * wide + p * piece) // columns
            slot = lax.rem(b * per_block + p, per_owner)
            k = lax.rem(owner // 2 - t // 2 + chips, chips)
            lane = lax.rem(owner, 2) == core

            @pl.loop(0, 2)
            def _(turn):
                r = 1 - turn
                at = pl.ds(pl.multiple_of(r * rows, rows), rows)
                weight = full[DOWN][b][:, p * piece : (p + 1) * piece]
                part[at, pl.ds(start, piece)] = jnp.dot(
                    hidden[at, :], weight, preferred_element_type=F32
                ).astype(BF16)

                @pl.when(jnp.logical_not(lane))
                def _():
                    down_to_pair(r, k, slot, start).start()

            @pl.when(lane & (k > 0))
            def _():
                for r in (1, 0):
                    down_to_pair(r, k, slot, start).wait_recv()
                    inside = pl.ds(pl.multiple_of(slot * piece, 128), piece)

                    @pl.loop(0, rows // 64)
                    def _(i):
                        here = pl.ds(pl.multiple_of(i * 64, 64), 64)
                        at = pl.ds(pl.multiple_of(r * rows + i * 64, 64), 64)
                        both = part[at, pl.ds(start, piece)].astype(F32) + pair_recv[r, k, here, inside].astype(F32)
                        part[at, pl.ds(start, piece)] = both.astype(BF16)

                    down_to_far(r, k, slot, start).start()

    def square_copy(r, k, peer):
        return pltpu.make_async_remote_copy(
            src_ref=sq_send.at[r], dst_ref=sq_recv.at[r, k - 1], send_sem=sq_ss.at[r, k - 1],
            recv_sem=sq_rs.at[r, k - 1], device_id={"tp": peer}, device_id_type=MESH,
        )

    def squares_send(r):
        for slot in range(per_owner):
            down_to_pair(r, 0, slot, 0).wait_recv()
            for k in range(1, chips):
                down_to_far(r, k, slot, 0).wait_recv()

        @pl.loop(0, seqs)
        def _(i):
            at, total = summed(r, i * length, length)
            second = first_full[at, own_columns(t)].astype(F32) + total
            squares = jnp.sum(second * second, axis=1, keepdims=True)
            sq_send[r, i] = jnp.transpose(jnp.broadcast_to(squares, (length, length)))[:8, :]

        for k in range(1, n_tp):
            square_copy(r, k, lax.rem(t + k, n_tp)).start()

    def close(r, dst):
        for k in range(1, n_tp):
            square_copy(r, k, lax.rem(t + n_tp - k, n_tp)).wait_recv()
        gain = out_gain[:, own_columns(t)]

        @pl.loop(0, seqs)
        def _(i):
            at, total = summed(r, i * length, length)
            second = first_full[at, own_columns(t)].astype(F32) + total
            squares = sq_send[r, i]
            for k in range(1, n_tp):
                squares = squares + sq_recv[r, k - 1, i]
            factor = column(lax.rsqrt(squares[:1, :] / width + 1e-06))
            inside = pl.ds(pl.multiple_of(i * length, length), length)
            dst[inside, :] = (second * factor * gain).astype(BF16)

    guest = lax.select(f == 1, 0, n - 1)
    has_guest = (f == 1) | (f == n - 2)
    inner = lax.select(f == 0, 1, n - 2)

    def tokens_in(device):
        return pltpu.make_async_remote_copy(
            src_ref=tok_ref, dst_ref=block_of(tok_full, 1, t), send_sem=guest_sem.at[0], recv_sem=guest_sem.at[1],
            device_id={"fs": device}, device_id_type=MESH,
        )

    def result_out(device):
        return pltpu.make_async_remote_copy(
            src_ref=returned, dst_ref=returned, send_sem=guest_sem.at[2], recv_sem=guest_sem.at[3],
            device_id={"fs": device}, device_id_type=MESH,
        )

    @pl.when(jnp.logical_not(is_host))
    def _():
        def halves(w, wait):
            @pl.loop(0, chunk_counts[w])
            def _(c):
                for k in range(1, parts):
                    if wait:
                        other_half(w, c, k).wait_send()
                    else:
                        other_half(w, c, k).start()

        tokens_in(inner).start()
        for w in range(MIXER):
            start_own(w)
        for w in range(MIXER):
            halves(w, False)
        for w in range(MIXER, 7):
            start_own(w)
            halves(w, False)
        tokens_in(inner).wait_send()
        for w in range(7):
            halves(w, True)

            @pl.loop(0, chunk_counts[w])
            def _(c):
                src = own[w].at[span(w, g, c), :]

                @pl.when(f == 0)
                def _():
                    z_copy(w, c, f, src, 1).wait_send()

                @pl.when(f == n - 1)
                def _():
                    z_copy(w, c, f, src, -1).wait_send()

        result_out(inner).wait_recv()
        out_ref[...] = returned[...]

    @pl.when(is_host)
    def _():
        own_tokens = pltpu.make_async_copy(tok_ref, block_of(tok_full, 0, t), own_sem.at[7])
        own_tokens.start()
        for w in range(MIXER):
            start_own(w)
        for w in range(7):
            own_copy(w).start()
        own_tokens.wait()
        gather_send(tok_full, 0, 0)
        steps = range(n - 2)
        for s in steps:
            receive(0, s)

        @pl.when(has_guest)
        def _():
            tokens_in(guest).wait_recv()

        gather_send(tok_full, 0, 1)
        gather_relay(tok_full, 0, 0)
        for w in range(1, MIXER):
            for s in steps:
                receive(w, s)
        start_own(GATE)
        gather_finish(tok_full, 0, 0)
        norm_rows(tok_full, mix_gain, 0)
        for w in range(MIXER):
            own_copy(w).wait()
            for s in steps:
                finish(w, s)
        mixer(0)
        sum_send(0)
        gather_relay(tok_full, 0, 1)
        receive(GATE, 0)
        start_own(UP)
        gather_finish(tok_full, 0, 1)
        norm_rows(tok_full, mix_gain, 1)
        sum_relay(0)
        mixer(1)
        sum_send(1)
        first_rows(0)
        gather_send(first_full, 2, 0)
        sum_relay(1)
        for s in steps[1:]:
            receive(GATE, s)
        receive(UP, 0)
        start_own(DOWN)
        gather_relay(first_full, 2, 0)
        first_rows(1)
        gather_send(first_full, 2, 1)
        gather_finish(first_full, 2, 0)
        norm_rows(first_full, ffn_gain, 0)
        for s in steps[1:]:
            receive(UP, s)
        gather_relay(first_full, 2, 1)
        for w in (GATE, UP):
            own_copy(w).wait()
            for s in steps:
                finish(w, s)
        hidden_rows(0)
        receive(DOWN, 0)
        gather_finish(first_full, 2, 1)
        norm_rows(first_full, ffn_gain, 1)
        hidden_rows(1)
        for r in range(2):
            for k in range(chips):
                to_pair(r, k).wait_send()
            for k in range(1, chips):
                to_far(r, k).wait_send()
        own_copy(DOWN).wait()
        down_block(f)

        for s in steps:
            if s > 0:
                receive(DOWN, s)
            finish(DOWN, s)

            @pl.loop(0, 2)
            def _(side):
                b = lax.select(side == 0, f - 1 - s, f + 1 + s)

                @pl.when((b >= 0) & (b < n))
                def _():
                    down_block(b)

        squares_send(1)
        squares_send(0)
        close(1, returned)

        @pl.when(has_guest)
        def _():
            result_out(guest).start()

        close(0, out_ref)

        @pl.when(has_guest)
        def _():
            result_out(guest).wait_send()

        for r in range(2):
            gather_sent(tok_full, 0, r)
            gather_sent(first_full, 2, r)
            for k in range(1, n_tp):
                square_copy(r, k, lax.rem(t + k, n_tp)).wait_send()
            for slot in range(per_owner):
                for k in range(chips):
                    down_to_pair(r, k, slot, 0).wait_send()
                for k in range(1, chips):
                    down_to_far(r, k, slot, 0).wait_send()
        for w in range(7):
            @pl.loop(0, chunk_counts[w])
            def _(c):
                @pl.loop(0, n)
                def _(blk):
                    here = region(w, blk, g, c)

                    @pl.when((f + 1 <= last_host) & (blk <= f))
                    def _():
                        z_copy(w, c, blk, here, 1).wait_send()

                    @pl.when((f - 1 >= first_host) & (blk >= f))
                    def _():
                        z_copy(w, c, blk, here, -1).wait_send()

                    whole = ((blk == 0) & (f == 1)) | ((blk == n - 1) & (f == n - 2))

                    @pl.when((blk != f) & jnp.logical_not(whole))
                    def _():
                        for k in range(1, parts):
                            y_copy(w, c, blk, g, k, y_peer(k)).wait_send()


def solution(mesh):
    n, parts, n_tp = mesh.shape["fs"], mesh.shape["grp"], mesh.shape["tp"]

    def local(tokens, mix_gain, outer, inner, value, taps, mix_out, ffn_gain, gate, up, down, out_gain):
        seqs, length, columns = tokens.shape
        rows, width = seqs * length, columns * n_tp
        weights = (outer, inner, value, mix_out, gate, up, down)
        counts = tuple(1 if w < MIXER else chunks_of(a.shape[0] // parts) for w, a in enumerate(weights))
        slots = sum(counts)
        channels, units = outer.shape[1], gate.shape[1]
        others, y_others = max(n_tp - 1, 1), max(parts - 1, 1)
        per_owner = columns // min(down.shape[1], columns)
        dma = pltpu.SemaphoreType.DMA
        scratch = [pltpu.VMEM((n,) + a.shape, BF16) for a in weights]
        chips = n_tp // 2
        scratch += [
            pltpu.VMEM((2 * rows, width), BF16),
            pltpu.VMEM((2 * rows, width), BF16),
            pltpu.VMEM((3, rows, channels), BF16),
            pltpu.VMEM((rows, channels), BF16),
            pltpu.VMEM((2 * rows, width), BF16),
            pltpu.VMEM((2, chips, rows, columns), BF16),
            pltpu.VMEM((2, chips, rows, columns), BF16),
            pltpu.VMEM((2 * rows, width), BF16),
            pltpu.VMEM((2 * rows, units), BF16),
            pltpu.VMEM((rows, columns), BF16),
            pltpu.VMEM((2, seqs, 8, length), F32),
            pltpu.VMEM((2, others, seqs, 8, length), F32),
            dma((slots, n)), dma((slots, n)), dma((slots, n)),
            dma((slots, n, y_others)), dma((slots, n, y_others)),
            dma((8,)), dma((3, 2, chips)), dma((3, 2, chips)), dma((3, 2, chips)), dma((3, 2, chips)),
            dma((2, chips, per_owner)), dma((2, chips, per_owner)),
            dma((2, chips, per_owner)), dma((2, chips, per_owner)),
            dma((2, others)), dma((2, others)), dma((4,)),
        ]
        out = pl.pallas_call(
            functools.partial(kernel, n, parts, n_tp, length, counts),
            out_shape=jax.ShapeDtypeStruct((rows, columns), BF16),
            in_specs=[pl.BlockSpec(memory_space=pltpu.VMEM)] * 12,
            out_specs=pl.BlockSpec(memory_space=pltpu.VMEM),
            scratch_shapes=scratch,
            compiler_params=pltpu.CompilerParams(
                collective_id=0, has_side_effects=True, vmem_limit_bytes=62 * 1024 * 1024
            ),
        )(
            tokens.reshape(rows, columns), mix_gain[None], outer, inner, value, taps, mix_out,
            ffn_gain[None], gate, up, down, out_gain[None],
        )
        return out.reshape(seqs, length, columns)

    in_specs = (
        P(("grp", "fs"), None, "tp"), P(), P("fs", "tp"), P("fs", "tp"), P("fs", "tp"), P(), P("tp", "fs"),
        P(), P("fs", "tp"), P("fs", "tp"), P("tp", "fs"), P(),
    )
    out_specs = P(("grp", "fs"), None, "tp")
    return jax.shard_map(local, mesh=mesh, in_specs=in_specs, out_specs=out_specs, check_vma=False)
```

profile of v0, /device:TPU:16, one launch (start us, length us, event | category | flops | bytes accessed | tf_op | source)
XLA Modules:
  0.0 200.2 jit_solution(16337063646021104136)
XLA Ops:
  0.0 198.4 %shard_map.118 = bf16[512,512]{1,0:T(8,128)(2,1)} custom-call(bf16[512,512]{1,0:T(8,128)(2,1)} %bitcast.6, f32[1,2048]{1,0:T(1,128)} %bitcast.7, bf16[512,256]{1,0:T(8,128)(2,1)} %w0.1, bf16[512,256]{1,0:T(8,128)(2,1)} %w1.1, bf16[512,256]{1,0:T(8,128)(2,1)} %w2.1, f32[3,1024]{1,0:T(4,128)} %taps_ref.1, bf16[256,512]{1,0:T(8,128)(2,1)} %w3.1, ...), custom_call_target="tpu_custom_call" | custom-call | tf_op jit(solution)/shard_map/pallas_call | solution.py:622
  198.4 1.9 copy.14
where the time goes:
time: 200 us
  Pallas kernels  198 us (99%)
    pallas_call x1, Pallas kernels, local(): pl.pallas_call(functools.partial(kernel, n, parts, n_tp, length, counts),...  198 us

commit v1 on v0

v1 whole, which is shorter than its diff:
```python
import functools

import jax
import jax.numpy as jnp
from jax import lax
from jax.experimental import pallas as pl
from jax.experimental.pallas import tpu as pltpu
from jax.sharding import PartitionSpec as P

MESH = pl.DeviceIdType.MESH
F32 = jnp.float32
BF16 = jnp.bfloat16
MIXER = 4
GATE, UP, DOWN = 4, 5, 6
SHARED = 2
LAG = 2


def tiles_of(units):
    if units % 128:
        return ((0, units),)
    return tuple((start, min(256, units - start)) for start in range(0, units, 256))


def column(rows):
    wide = jnp.broadcast_to(rows, (rows.shape[1], rows.shape[1]))
    return jnp.transpose(wide)[:, :1]


def kernel(
    n, parts, n_tp, length, spans,
    tok_ref, mix_gain, w0, w1, w2, taps_ref, w3, ffn_gain, w4, w5, w6, out_gain,
    out_ref,
    f0, f1, f2, f3, f4, f5, f6,
    tok_full, normed, proj, gated, part, pair_recv, far_recv, first_full, hidden, returned, second_own, sq_acc,
    sq_send, sq_recv, sq_total, sq_back,
    z_send, z_recv, y_send, y_recv, own_sem, pair_ss, pair_rs, far_ss, far_rs,
    down_pair_ss, down_pair_rs, down_far_ss, down_far_rs, sq_ss, sq_rs, back_ss, back_rs, guest_sem,
):
    own = (w0, w1, w2, w3, w4, w5, w6)
    full = (f0, f1, f2, f3, f4, f5, f6)
    f, g, t = lax.axis_index("fs"), lax.axis_index("grp"), lax.axis_index("tp")
    rows, columns = tok_ref.shape
    width = columns * n_tp
    seqs = rows // length
    counts = [len(tiles) for tiles in spans]
    bases = [sum(counts[:w]) for w in range(7)]

    def y_peer(k):
        return lax.rem(g + k, parts)

    def tp_peer(k):
        return lax.rem(t + k, n_tp)

    def span(w, half, c):
        size = own[w].shape[0] // parts
        if isinstance(c, int):
            at = pl.ds(*spans[w][c])
        else:
            width_c = spans[w][0][1]
            at = pl.ds(pl.multiple_of(c * width_c, 128), width_c)
        return pl.ds(pl.multiple_of(half * size, 8), size), at

    def region(w, blk, half, c):
        at_rows, at_cols = span(w, half, c)
        return full[w].at[blk, at_rows, at_cols]

    def piece_of(w, half, c):
        at_rows, at_cols = span(w, half, c)
        return own[w].at[at_rows, at_cols]

    barrier = pltpu.get_barrier_semaphore()
    for k in range(1, n_tp):
        pl.semaphore_signal(barrier, inc=1, device_id={"tp": tp_peer(k)}, device_id_type=MESH)
    for k in range(1, parts):
        pl.semaphore_signal(barrier, inc=1, device_id={"grp": y_peer(k)}, device_id_type=MESH)

    @pl.when(f < n - 1)
    def _():
        pl.semaphore_signal(barrier, inc=1, device_id={"fs": f + 1}, device_id_type=MESH)

    @pl.when(f > 0)
    def _():
        pl.semaphore_signal(barrier, inc=1, device_id={"fs": f - 1}, device_id_type=MESH)

    neighbours = lax.min(f, 1) + lax.min(n - 1 - f, 1)
    pl.semaphore_wait(barrier, n_tp - 1 + parts - 1 + neighbours)

    def z_slot(blk, step):
        return lax.select((blk == f) & (step < 0), n, blk)

    def half_block(w, blk):
        size = own[w].shape[0] // parts
        return full[w].at[blk, pl.ds(pl.multiple_of(g * size, 8), size), :]

    def z_sent(w, blk, step):
        half = half_block(w, blk)
        pltpu.make_async_remote_copy(
            src_ref=half, dst_ref=half, send_sem=z_send.at[w, z_slot(blk, step)], recv_sem=z_recv.at[bases[w], blk],
            device_id={"fs": f + step}, device_id_type=MESH,
        ).wait_send()

    def y_sent(w, blk, k):
        half = half_block(w, blk)
        pltpu.make_async_remote_copy(
            src_ref=half, dst_ref=half, send_sem=y_send.at[w, blk, k - 1], recv_sem=y_recv.at[bases[w], blk, k - 1],
            device_id={"grp": y_peer(k)}, device_id_type=MESH,
        ).wait_send()

    def z_copy(w, c, blk, src, step):
        return pltpu.make_async_remote_copy(
            src_ref=src, dst_ref=region(w, blk, g, c),
            send_sem=z_send.at[w, z_slot(blk, step)], recv_sem=z_recv.at[bases[w] + c, blk],
            device_id={"fs": f + step}, device_id_type=MESH,
        )

    def y_copy(w, c, blk, half, k, peer):
        return pltpu.make_async_remote_copy(
            src_ref=region(w, blk, half, c), dst_ref=region(w, blk, half, c),
            send_sem=y_send.at[w, blk, k - 1], recv_sem=y_recv.at[bases[w] + c, blk, k - 1],
            device_id={"grp": peer}, device_id_type=MESH,
        )

    first_host, last_host = 1, n - 2
    is_host = (f >= first_host) & (f <= last_host)
    inner = lax.select(2 * f + 1 < n, 1, -1)

    def start_own(w, c):
        src = piece_of(w, g, c)

        @pl.when(f + 1 <= last_host)
        def _():
            z_copy(w, c, f, src, 1).start()

        @pl.when(f - 1 >= first_host)
        def _():
            z_copy(w, c, f, src, -1).start()

    def other_half(w, c, k):
        half = lax.rem(g + parts - k, parts)
        inward = lax.select(f == 0, 1, n - 2)
        return pltpu.make_async_remote_copy(
            src_ref=piece_of(w, half, c), dst_ref=region(w, f, half, c),
            send_sem=y_send.at[w, f, k - 1], recv_sem=y_recv.at[bases[w] + c, f, k - 1],
            device_id={"fs": inward}, device_id_type=MESH,
        )

    def direct(w):
        return w >= SHARED

    def relay(w, c, s, toward, next_to_edge):
        blk = f + toward * (1 + s)
        step = -toward

        @pl.when((blk >= 0) & (blk < n))
        def _():
            z_copy(w, c, blk, region(w, blk, g, c), step).wait_recv()

            def share():
                for k in range(1, parts):
                    y_copy(w, c, blk, g, k, y_peer(k)).start()

            def onward():
                z_copy(w, c, blk, region(w, blk, g, c), step).start()

            pl.when((f + step <= last_host) & (f + step >= first_host))(onward)
            if next_to_edge and direct(w):
                pl.when((blk > 0) & (blk < n - 1))(share)
            else:
                share()

    def from_inner(w, c):
        relay(w, c, 0, inner, True)

    def from_outer(w, c):
        relay(w, c, 0, -inner, True)

    def from_far(w, c):
        @pl.loop(1, n - 2)
        def _(s):
            relay(w, c, s, inner, False)
            relay(w, c, s, -inner, False)

    def finish(w, c, blk):
        for k in range(1, parts):
            source = lax.rem(g + parts - k, parts)
            y_copy(w, c, blk, source, k, source).wait_recv()

    def finish_all(w, c):
        @pl.loop(0, n)
        def _(blk):
            pl.when(blk != f)(lambda: finish(w, c, blk))

    def own_copy(w):
        return pltpu.make_async_copy(own[w], full[w].at[f], own_sem.at[w])

    def own_columns(owner):
        return pl.ds(pl.multiple_of(owner * columns, 128), columns)

    chips = n_tp // 2
    core = lax.rem(t, 2)
    pair = t + 1 - 2 * core

    def ahead(k, start=None):
        return lax.rem((t if start is None else start) + 2 * k, n_tp)

    def behind(k, start=None):
        return lax.rem((t if start is None else start) + n_tp - 2 * k, n_tp)

    def set_rows(r):
        return pl.ds(r * rows, rows)

    def pair_copy(stage, r, k, src, dst):
        return pltpu.make_async_remote_copy(
            src_ref=src, dst_ref=dst, send_sem=pair_ss.at[stage, r, k], recv_sem=pair_rs.at[stage, r, k],
            device_id={"tp": pair}, device_id_type=MESH,
        )

    def far_copy(stage, r, k, src, dst, peer):
        return pltpu.make_async_remote_copy(
            src_ref=src, dst_ref=dst, send_sem=far_ss.at[stage, r, k], recv_sem=far_rs.at[stage, r, k],
            device_id={"tp": peer}, device_id_type=MESH,
        )

    def block_of(buf, r, owner):
        return buf.at[set_rows(r), own_columns(owner)]

    def gather_send(buf, stage, r):
        mine = block_of(buf, r, t)
        for k in range(1, chips):
            far_copy(stage, r, k, mine, mine, ahead(k)).start()
        pair_copy(stage, r, 0, mine, mine).start()

    def gather_relay(buf, stage, r):
        for k in range(1, chips):
            theirs = block_of(buf, r, behind(k))
            far_copy(stage, r, k, theirs, theirs, behind(k)).wait_recv()
            pair_copy(stage, r, k, theirs, theirs).start()

    def gather_finish(buf, stage, r):
        for k in range(chips):
            theirs = block_of(buf, r, behind(k, pair))
            pair_copy(stage, r, k, theirs, theirs).wait_recv()

    def gather_sent(buf, stage, r):
        mine = block_of(buf, r, t)
        for k in range(1, chips):
            far_copy(stage, r, k, mine, mine, ahead(k)).wait_send()
        for k in range(chips):
            pair_copy(stage, r, k, mine, mine).wait_send()

    def to_pair(r, k):
        return pair_copy(1, r, k, block_of(part, r, ahead(k, pair)), pair_recv.at[r, k])

    def to_far(r, k):
        return far_copy(1, r, k, block_of(part, r, ahead(k)), far_recv.at[r, k], ahead(k))

    def sum_send(r):
        for k in range(chips - 1, -1, -1):
            to_pair(r, k).start()

    def sum_relay(r):
        for k in range(1, chips):
            to_pair(r, k).wait_recv()

            @pl.loop(0, rows // 64)
            def _(i):
                inside = pl.ds(pl.multiple_of(i * 64, 64), 64)
                at = pl.ds(pl.multiple_of(r * rows + i * 64, 64), 64)
                both = part[at, own_columns(ahead(k))].astype(F32) + pair_recv[r, k, inside, :].astype(F32)
                part[at, own_columns(ahead(k))] = both.astype(BF16)

            to_far(r, k).start()

    def summed(r, start, size):
        inside = pl.ds(pl.multiple_of(start, size), size)
        at = pl.ds(pl.multiple_of(r * rows + start, size), size)
        total = part[at, own_columns(t)].astype(F32) + pair_recv[r, 0, inside, :].astype(F32)
        for k in range(1, chips):
            total = total + far_recv[r, k, inside, :].astype(F32)
        return at, total

    def first_rows(r):
        to_pair(r, 0).wait_recv()
        for k in range(1, chips):
            to_far(r, k).wait_recv()

        @pl.loop(0, rows // 64)
        def _(i):
            at, total = summed(r, i * 64, 64)
            first_full[at, own_columns(t)] = (tok_full[at, own_columns(t)].astype(F32) + total).astype(BF16)

    def norm_rows(source, gain, r):
        size = 32

        @pl.loop(0, rows // size)
        def _(i):
            at = pl.ds(pl.multiple_of(r * rows + i * size, size), size)
            values = source[at, :].astype(F32)
            scale = lax.rsqrt(jnp.sum(values * values, axis=1, keepdims=True) / width + 1e-06)
            normed[at, :] = (values * scale * gain[...]).astype(BF16)

    channels = w0.shape[1]
    block = w3.shape[1]
    units = w4.shape[1]
    tap_count = taps_ref.shape[0]

    def mixer(r):
        for w in range(3):
            weight = full[w][...].reshape(width, channels)
            proj[w] = jnp.dot(normed[set_rows(r), :], weight, preferred_element_type=F32).astype(BF16)
        taps = taps_ref[:, pl.ds(pl.multiple_of(t * channels, 128), channels)]

        @pl.loop(0, seqs)
        def _(i):
            at = pl.ds(pl.multiple_of(i * length, length), length)
            product = proj[1, at, :].astype(F32) * proj[2, at, :].astype(F32)
            position = lax.broadcasted_iota(jnp.int32, product.shape, 0)
            conv = jnp.zeros_like(product)
            for offset in range(tap_count):
                shift = tap_count - 1 - offset
                moved = product if shift == 0 else jnp.where(position >= shift, pltpu.roll(product, shift, 0), 0.0)
                conv = conv + taps[offset : offset + 1, :] * moved
            gated[at, :] = (proj[0, at, :].astype(F32) * conv).astype(BF16)

        @pl.loop(0, n)
        def _(b):
            at = pl.ds(pl.multiple_of(b * block, 128), block)
            part[set_rows(r), at] = jnp.dot(gated[...], full[3][b], preferred_element_type=F32).astype(BF16)

    def hidden_tile(r, start, size):
        at = pl.ds(start, size)
        left = normed[set_rows(r), :]
        gate = jnp.dot(left, full[GATE][:, :, at].reshape(width, size), preferred_element_type=F32)
        upward = jnp.dot(left, full[UP][:, :, at].reshape(width, size), preferred_element_type=F32)
        hidden[set_rows(r), at] = (gate / (1.0 + jnp.exp(-gate)) * upward).astype(BF16)

    def hidden_tiles(c, r):
        first, total = spans[GATE][c]
        for offset in range(0, total, 256):
            hidden_tile(r, first + offset, min(256, total - offset))

    wide = w6.shape[1]
    piece = spans[DOWN][0][1]
    pieces = counts[DOWN]

    def down_to_pair(r, k, slot, start):
        inside = pl.ds(pl.multiple_of(slot * piece, 128), piece)
        return pltpu.make_async_remote_copy(
            src_ref=part.at[set_rows(r), pl.ds(start, piece)], dst_ref=pair_recv.at[r, k, :, inside],
            send_sem=down_pair_ss.at[r, k], recv_sem=down_pair_rs.at[r, k, slot],
            device_id={"tp": pair}, device_id_type=MESH,
        )

    def down_to_far(r, k, slot, start):
        inside = pl.ds(pl.multiple_of(slot * piece, 128), piece)
        return pltpu.make_async_remote_copy(
            src_ref=part.at[set_rows(r), pl.ds(start, piece)], dst_ref=far_recv.at[r, k, :, inside],
            send_sem=down_far_ss.at[r, k], recv_sem=down_far_rs.at[r, k, slot],
            device_id={"tp": lax.rem(t + 2 * k, n_tp)}, device_id_type=MESH,
        )

    def down_sent(r, k):
        whole = pair_recv.at[r, k]
        pltpu.make_async_remote_copy(
            src_ref=whole, dst_ref=whole, send_sem=down_pair_ss.at[r, k], recv_sem=down_pair_rs.at[r, k, 0],
            device_id={"tp": pair}, device_id_type=MESH,
        ).wait_send()
        if k > 0:
            pltpu.make_async_remote_copy(
                src_ref=whole, dst_ref=whole, send_sem=down_far_ss.at[r, k], recv_sem=down_far_rs.at[r, k, 0],
                device_id={"tp": lax.rem(t + 2 * k, n_tp)}, device_id_type=MESH,
            ).wait_send()

    def place(b, c):
        start = pl.multiple_of(b * wide + c * piece, 128)
        owner = (b * wide + c * piece) // columns
        slot = lax.rem(b * wide + c * piece, columns) // piece
        k = lax.rem(owner // 2 - t // 2 + chips, chips)
        return start, owner, slot, k, lax.rem(owner, 2) == core

    def down_product(b, offset, size):
        at_cols = pl.ds(pl.multiple_of(b * wide + offset, 128), size)

        @pl.loop(0, 2)
        def _(turn):
            r = 1 - turn
            at = pl.ds(pl.multiple_of(r * rows, rows), rows)
            weight = full[DOWN][b, :, pl.ds(offset, size)]
            part[at, at_cols] = jnp.dot(hidden[at, :], weight, preferred_element_type=F32).astype(BF16)

    def to_lane(b, c):
        start, owner, slot, k, lane = place(b, c)

        @pl.when(jnp.logical_not(lane))
        def _():
            for r in (1, 0):
                down_to_pair(r, k, slot, start).start()

    def combine(b, c):
        start, owner, slot, k, lane = place(b, c)

        @pl.when(lane & (k > 0))
        def _():
            inside = pl.ds(pl.multiple_of(slot * piece, 128), piece)
            for r in (1, 0):
                down_to_pair(r, k, slot, start).wait_recv()

                @pl.loop(0, rows // 64)
                def _(i):
                    here = pl.ds(pl.multiple_of(i * 64, 64), 64)
                    at = pl.ds(pl.multiple_of(r * rows + i * 64, 64), 64)
                    both = part[at, pl.ds(start, piece)].astype(F32) + pair_recv[r, k, here, inside].astype(F32)
                    part[at, pl.ds(start, piece)] = both.astype(BF16)

                down_to_far(r, k, slot, start).start()

    def back_copy(slot, device):
        at = pl.ds(pl.multiple_of(slot * piece, 128), piece)
        return pltpu.make_async_remote_copy(
            src_ref=returned.at[:, at], dst_ref=returned.at[:, at], send_sem=back_ss.at[0], recv_sem=back_rs.at[slot],
            device_id={"fs": device}, device_id_type=MESH,
        )

    def back_sent():
        pltpu.make_async_remote_copy(
            src_ref=returned, dst_ref=returned, send_sem=back_ss.at[0], recv_sem=back_rs.at[0],
            device_id={"fs": guest}, device_id_type=MESH,
        ).wait_send()

    def settle(b, c):
        start, owner, slot, k, lane = place(b, c)

        @pl.when(owner == t)
        def _():
            inside = pl.ds(pl.multiple_of(slot * piece, 128), piece)
            for r in (1, 0):
                down_to_pair(r, 0, slot, start).wait_recv()
                for far in range(1, chips):
                    down_to_far(r, far, slot, start).wait_recv()

                @pl.loop(0, rows // 64)
                def _(i):
                    here = pl.ds(pl.multiple_of(i * 64, 64), 64)
                    at = pl.ds(pl.multiple_of(r * rows + i * 64, 64), 64)
                    total = part[at, pl.ds(start, piece)].astype(F32) + pair_recv[r, 0, here, inside].astype(F32)
                    for far in range(1, chips):
                        total = total + far_recv[r, far, here, inside].astype(F32)
                    second = first_full[at, pl.ds(start, piece)].astype(F32) + total
                    squares = second * second
                    folded = squares[:, :128]
                    for lane_block in range(1, piece // 128):
                        folded = folded + squares[:, lane_block * 128 : (lane_block + 1) * 128]
                    sq_acc[at, :] += folded
                    if r == 0:
                        second_own[here, inside] = second
                    else:
                        returned[here, inside] = second.astype(BF16)

                if r == 1:
                    pl.when(has_guest)(lambda: back_copy(slot, guest).start())

    def square_copy(r, k, peer):
        return pltpu.make_async_remote_copy(
            src_ref=sq_send.at[r], dst_ref=sq_recv.at[r, k - 1], send_sem=sq_ss.at[r, k - 1],
            recv_sem=sq_rs.at[r, k - 1], device_id={"tp": peer}, device_id_type=MESH,
        )

    def squares_send(r):
        @pl.loop(0, seqs)
        def _(i):
            at = pl.ds(pl.multiple_of(r * rows + i * length, length), length)
            squares = jnp.sum(sq_acc[at, :], axis=1, keepdims=True)
            sq_send[r, i] = jnp.transpose(jnp.broadcast_to(squares, (length, length)))[:8, :]

        for k in range(1, n_tp):
            square_copy(r, k, lax.rem(t + k, n_tp)).start()

    def squares_total(r):
        for k in range(1, n_tp):
            square_copy(r, k, lax.rem(t + n_tp - k, n_tp)).wait_recv()
        total = sq_send[r]
        for k in range(1, n_tp):
            total = total + sq_recv[r, k - 1]
        return total

    def close(values, squares_of):
        gain = out_gain[:, own_columns(t)]

        @pl.loop(0, seqs)
        def _(i):
            factor = column(lax.rsqrt(squares_of[i][:1, :] / width + 1e-06))
            inside = pl.ds(pl.multiple_of(i * length, length), length)
            out_ref[inside, :] = (values[inside, :].astype(F32) * factor * gain).astype(BF16)

    def squares_back(device):
        return pltpu.make_async_remote_copy(
            src_ref=sq_back, dst_ref=sq_back, send_sem=guest_sem.at[2], recv_sem=guest_sem.at[3],
            device_id={"fs": device}, device_id_type=MESH,
        )

    guest = lax.select(f == 1, 0, n - 1)
    has_guest = (f == 1) | (f == n - 2)
    inward = lax.select(f == 0, 1, n - 2)

    def tokens_in(device):
        return pltpu.make_async_remote_copy(
            src_ref=tok_ref, dst_ref=block_of(tok_full, 1, t), send_sem=guest_sem.at[0], recv_sem=guest_sem.at[1],
            device_id={"fs": device}, device_id_type=MESH,
        )

    @pl.when(jnp.logical_not(is_host))
    def _():
        order = [("own", w, 0) for w in range(MIXER)] + [("tokens", 0, 0)]
        order += [("other", w, 0) for w in range(MIXER) if direct(w)]
        for c in range(counts[GATE]):
            order += [("own", GATE, c), ("own", UP, c), ("other", GATE, c), ("other", UP, c)]
        for kind in ("own", "other"):
            order += [(kind, DOWN, c) for c in range(pieces)]
        for kind, w, c in order:
            if kind == "own":
                start_own(w, c)
            elif kind == "tokens":
                tokens_in(inward).start()
            else:
                for k in range(1, parts):
                    other_half(w, c, k).start()
        tokens_in(inward).wait_send()
        for w in range(7):
            z_sent(w, f, lax.select(f == 0, 1, -1))
            if direct(w):
                for k in range(1, parts):
                    y_sent(w, f, k)
        for slot in range(columns // piece):
            back_copy(slot, inward).wait_recv()
        squares_back(inward).wait_recv()
        close(returned, sq_back)

    @pl.when(is_host)
    def _():
        own_tokens = pltpu.make_async_copy(tok_ref, block_of(tok_full, 0, t), own_sem.at[7])
        own_tokens.start()
        for w in range(MIXER):
            start_own(w, 0)
        for w in range(7):
            own_copy(w).start()
        own_tokens.wait()
        gather_send(tok_full, 0, 0)
        sq_acc[...] = jnp.zeros_like(sq_acc)
        for w in range(MIXER):
            from_inner(w, 0)
            from_outer(w, 0)
        last = counts[GATE] - 1

        def start_pair(c):
            if c <= last:
                start_own(GATE, c)
                start_own(UP, c)

        def inner_pair(c):
            if c <= last:
                from_inner(GATE, c)
                from_inner(UP, c)

        def outer_pair(c):
            if c <= last:
                from_outer(GATE, c)
                from_outer(UP, c)

        def far_pair(c):
            if c <= last:
                from_far(GATE, c)
                from_far(UP, c)

        def start_down(first, end):
            for c in range(first, min(end, pieces)):
                start_own(DOWN, c)

        def inner_down(c):
            if c < pieces:
                from_inner(DOWN, c)

        def outer_down(c):
            if c < pieces:
                from_outer(DOWN, c)

        def tile(c, r):
            if c <= last:
                if r == 0:
                    for w in (GATE, UP):
                        finish_all(w, c)
                hidden_tiles(c, r)

        def drain(group):
            for w in group:
                @pl.loop(0, n)
                def _(blk):
                    pl.when((f + 1 <= last_host) & (blk <= f))(lambda: z_sent(w, blk, 1))
                    pl.when((f - 1 >= first_host) & (blk >= f))(lambda: z_sent(w, blk, -1))
                    whole = ((blk == 0) & (f == 1)) | ((blk == n - 1) & (f == n - 2))
                    relayed = (blk != f) & jnp.logical_not(whole) if direct(w) else blk != f

                    @pl.when(relayed)
                    def _():
                        for k in range(1, parts):
                            y_sent(w, blk, k)

        start_pair(0)
        start_pair(1)
        gather_relay(tok_full, 0, 0)
        from_far(0, 0)
        gather_finish(tok_full, 0, 0)
        norm_rows(tok_full, mix_gain, 0)
        for w in range(1, MIXER):
            from_far(w, 0)

        @pl.when(has_guest)
        def _():
            tokens_in(guest).wait_recv()

        gather_send(tok_full, 0, 1)
        inner_pair(0)
        outer_pair(0)
        start_pair(2)
        for w in range(MIXER):
            own_copy(w).wait()
            finish_all(w, 0)
        mixer(0)
        sum_send(0)
        inner_pair(1)
        gather_relay(tok_full, 0, 1)
        sum_relay(0)
        gather_finish(tok_full, 0, 1)
        norm_rows(tok_full, mix_gain, 1)
        far_pair(0)
        mixer(1)
        sum_send(1)
        outer_pair(1)
        start_pair(3)
        sum_relay(1)
        inner_pair(2)
        first_rows(0)
        gather_send(first_full, 2, 0)
        far_pair(1)
        outer_pair(2)
        start_pair(4)
        inner_pair(3)
        first_rows(1)
        gather_send(first_full, 2, 1)
        far_pair(2)
        outer_pair(3)
        start_pair(5)
        inner_pair(4)
        for w in (GATE, UP):
            own_copy(w).wait()
        gather_relay(first_full, 2, 0)
        far_pair(3)
        gather_finish(first_full, 2, 0)
        norm_rows(first_full, ffn_gain, 0)
        outer_pair(4)
        start_down(0, 2)
        inner_pair(5)
        tile(0, 0)
        tile(1, 0)
        tile(2, 0)
        gather_relay(first_full, 2, 1)
        far_pair(4)
        outer_pair(5)
        start_down(2, pieces)
        gather_finish(first_full, 2, 1)
        norm_rows(first_full, ffn_gain, 1)
        for r in range(2):
            for k in range(chips):
                to_pair(r, k).wait_send()
            for k in range(1, chips):
                to_far(r, k).wait_send()
        tile(3, 0)
        inner_down(0)
        far_pair(5)
        tile(0, 1)
        outer_down(0)
        tile(1, 1)
        inner_down(1)
        tile(2, 1)
        outer_down(1)
        tile(3, 1)
        inner_down(2)
        tile(4, 0)
        tile(4, 1)
        outer_down(2)
        inner_down(3)
        tile(5, 0)
        tile(5, 1)
        for c in range(6, last + 1):
            start_pair(c)
            inner_pair(c)
            outer_pair(c)
            far_pair(c)
            tile(c, 0)
            tile(c, 1)
        for c in range(4, pieces):
            inner_down(c)
        own_copy(DOWN).wait()
        near = f + inner
        down_product(f, 0, wide)
        for c in range(pieces):
            to_lane(f, c)
        for c in range(3, pieces):
            outer_down(c)
        from_far(DOWN, 0)
        for c in range(pieces):
            finish(DOWN, c, near)
        down_product(near, 0, wide)
        for c in range(pieces):
            to_lane(near, c)
        for c in range(1, min(2, pieces)):
            from_far(DOWN, c)
        for c in range(pieces):
            combine(f, c)
        for c in range(2, min(3, pieces)):
            from_far(DOWN, c)
        for c in range(pieces):
            combine(near, c)
        drain(range(DOWN))
        for r in range(2):
            gather_sent(tok_full, 0, r)
            gather_sent(first_full, 2, r)
        for c in range(3, pieces):
            from_far(DOWN, c)

        def others(visit):
            @pl.loop(1, n - 2)
            def _(s):
                for toward in (inner, -inner):
                    b = f + toward * (1 + s)
                    pl.when((b >= 0) & (b < n))(lambda: visit(b))

        outer = f - inner

        def take(b, c):
            finish(DOWN, c, b)
            down_product(b, pl.multiple_of(c * piece, 128), piece)
            to_lane(b, c)

        @pl.loop(0, pieces)
        def _(c):
            others(lambda b: take(b, c))
            take(outer, c)
            others(lambda b: combine(b, c))
            combine(outer, c)

            @pl.when(c >= LAG)
            def _():
                others(lambda b: settle(b, c - LAG))
                settle(outer, c - LAG)

        @pl.loop(0, pieces)
        def _(i):
            settle(f, i)
            settle(near, i)

        for c in range(max(pieces - LAG, 0), pieces):
            others(lambda b: settle(b, c))
            settle(outer, c)

        squares_send(1)
        squares_send(0)
        sq_back[...] = squares_total(1)

        @pl.when(has_guest)
        def _():
            squares_back(guest).start()

        sq_total[...] = squares_total(0)
        close(second_own, sq_total)

        @pl.when(has_guest)
        def _():
            squares_back(guest).wait_send()
            back_sent()

        for r in range(2):
            for k in range(1, n_tp):
                square_copy(r, k, lax.rem(t + k, n_tp)).wait_send()
            for k in range(chips):
                down_sent(r, k)
        drain((DOWN,))


def solution(mesh):
    n, parts, n_tp = mesh.shape["fs"], mesh.shape["grp"], mesh.shape["tp"]

    def local(tokens, mix_gain, outer, inner, value, taps, mix_out, ffn_gain, gate, up, down, out_gain):
        seqs, length, columns = tokens.shape
        rows, width = seqs * length, columns * n_tp
        weights = (outer, inner, value, mix_out, gate, up, down)
        piece = min(down.shape[1], columns, 128)
        spans = [((0, a.shape[1]),) for a in weights]
        spans[GATE] = spans[UP] = tiles_of(gate.shape[1])
        spans[DOWN] = tuple((start, piece) for start in range(0, down.shape[1], piece))
        slots = sum(len(tiles) for tiles in spans)
        channels, units = outer.shape[1], gate.shape[1]
        others, y_others = max(n_tp - 1, 1), max(parts - 1, 1)
        per_owner = columns // piece
        dma = pltpu.SemaphoreType.DMA
        scratch = [pltpu.VMEM((n,) + a.shape, BF16) for a in weights]
        chips = n_tp // 2
        scratch += [
            pltpu.VMEM((2 * rows, width), BF16),
            pltpu.VMEM((2 * rows, width), BF16),
            pltpu.VMEM((3, rows, channels), BF16),
            pltpu.VMEM((rows, channels), BF16),
            pltpu.VMEM((2 * rows, width), BF16),
            pltpu.VMEM((2, chips, rows, columns), BF16),
            pltpu.VMEM((2, chips, rows, columns), BF16),
            pltpu.VMEM((2 * rows, width), BF16),
            pltpu.VMEM((2 * rows, units), BF16),
            pltpu.VMEM((rows, columns), BF16),
            pltpu.VMEM((rows, columns), F32),
            pltpu.VMEM((2 * rows, 128), F32),
            pltpu.VMEM((2, seqs, 8, length), F32),
            pltpu.VMEM((2, others, seqs, 8, length), F32),
            pltpu.VMEM((seqs, 8, length), F32),
            pltpu.VMEM((seqs, 8, length), F32),
            dma((7, n + 1)), dma((slots, n)),
            dma((7, n, y_others)), dma((slots, n, y_others)),
            dma((8,)), dma((3, 2, chips)), dma((3, 2, chips)), dma((3, 2, chips)), dma((3, 2, chips)),
            dma((2, chips)), dma((2, chips, per_owner)), dma((2, chips)), dma((2, chips, per_owner)),
            dma((2, others)), dma((2, others)), dma((1,)), dma((per_owner,)), dma((4,)),
        ]
        hbm, vmem = pl.BlockSpec(memory_space=pl.ANY), pl.BlockSpec(memory_space=pltpu.VMEM)
        out = pl.pallas_call(
            functools.partial(kernel, n, parts, n_tp, length, tuple(spans)),
            out_shape=jax.ShapeDtypeStruct((rows, columns), BF16),
            in_specs=[hbm, vmem, hbm, hbm, hbm, vmem, hbm, vmem, hbm, hbm, hbm, vmem],
            out_specs=pl.BlockSpec(memory_space=pltpu.VMEM),
            scratch_shapes=scratch,
            compiler_params=pltpu.CompilerParams(
                collective_id=0, has_side_effects=True, vmem_limit_bytes=62 * 1024 * 1024
            ),
        )(
            tokens.reshape(rows, columns), mix_gain[None], outer, inner, value, taps, mix_out,
            ffn_gain[None], gate, up, down, out_gain[None],
        )
        return out.reshape(seqs, length, columns)

    in_specs = (
        P(("grp", "fs"), None, "tp"), P(), P("fs", "tp"), P("fs", "tp"), P("fs", "tp"), P(), P("tp", "fs"),
        P(), P("fs", "tp"), P("fs", "tp"), P("tp", "fs"), P(),
    )
    out_specs = P(("grp", "fs"), None, "tp")
    return jax.shard_map(local, mesh=mesh, in_specs=in_specs, out_specs=out_specs, check_vma=False)
```

time: 200 us -> 163 us (0.81)
  the two profiles are of different devices: /device:TPU:16 before, /device:TPU:0 now
where the time goes in v1:
time: 163 us; the launch traced here: 162 us
  Pallas kernels  161 us (99%)
  local copies, waits for them, and re-layouts  1.87 us (1%)
    pallas_call x1, Pallas kernels, local(): pl.pallas_call(functools.partial(kernel, n, parts, n_tp, length, tuple(sp...  161 us

profile of v1, /device:TPU:0, one launch (start us, length us, event | category | flops | bytes accessed | tf_op | source)
XLA Modules:
  0.0 162.4 jit_solution(16623431865055284051)
XLA Ops:
  0.0 160.5 %shard_map.118 = bf16[512,512]{1,0:T(8,128)(2,1)} custom-call(bf16[512,512]{1,0:T(8,128)(2,1)} %bitcast.6, f32[1,2048]{1,0:T(1,128)} %bitcast.7, bf16[512,256]{1,0:T(8,128)(2,1)} %w0.1, bf16[512,256]{1,0:T(8,128)(2,1)} %w1.1, bf16[512,256]{1,0:T(8,128)(2,1)} %w2.1, f32[3,1024]{1,0:T(4,128)} %taps_ref.1, bf16[256,512]{1,0:T(8,128)(2,1)} %w3.1, ...), custom_call_target="tpu_custom_call" | custom-call | tf_op jit(solution)/shard_map/pallas_call | solution.py:832
  160.5 1.9 %copy.14 = bf16[4,128,512]{2,1,0:T(8,128)(2,1)} copy(bf16[4,128,512]{2,1,0:T(8,128)(2,1)} %bitcast.5) | data formatting | bytes 1048576

commit v2 on v1

--- a/solution.py
+++ b/solution.py
@@ -12,7 +12,7 @@
 BF16 = jnp.bfloat16
 MIXER = 4
 GATE, UP, DOWN = 4, 5, 6
-SHARED = 2
+SHARED = 1
 LAG = 2
 
 
@@ -29,11 +29,11 @@
 
 def kernel(
     n, parts, n_tp, length, spans,
-    tok_ref, mix_gain, w0, w1, w2, taps_ref, w3, ffn_gain, w4, w5, w6, out_gain,
+    tok_ref, mix_gain_in, w0, w1, w2, taps_in, w3, ffn_gain_in, w4, w5, w6, out_gain_in,
     out_ref,
     f0, f1, f2, f3, f4, f5, f6,
     tok_full, normed, proj, gated, part, pair_recv, far_recv, first_full, hidden, returned, second_own, sq_acc,
-    sq_send, sq_recv, sq_total, sq_back,
+    sq_send, sq_recv, sq_total, mix_gain, taps_ref, ffn_gain, out_gain,
     z_send, z_recv, y_send, y_recv, own_sem, pair_ss, pair_rs, far_ss, far_rs,
     down_pair_ss, down_pair_rs, down_far_ss, down_far_rs, sq_ss, sq_rs, back_ss, back_rs, guest_sem,
 ):
@@ -194,6 +194,10 @@
     def own_copy(w):
         return pltpu.make_async_copy(own[w], full[w].at[f], own_sem.at[w])
 
+    def small_copy(i):
+        pairs = ((mix_gain_in, mix_gain), (taps_in, taps_ref), (ffn_gain_in, ffn_gain), (out_gain_in, out_gain))
+        return pltpu.make_async_copy(*pairs[i], own_sem.at[8 + i])
+
     def own_columns(owner):
         return pl.ds(pl.multiple_of(owner * columns, 128), columns)
 
@@ -305,10 +309,11 @@
     units = w4.shape[1]
     tap_count = taps_ref.shape[0]
 
-    def mixer(r):
-        for w in range(3):
-            weight = full[w][...].reshape(width, channels)
-            proj[w] = jnp.dot(normed[set_rows(r), :], weight, preferred_element_type=F32).astype(BF16)
+    def project(w, r):
+        weight = full[w][...].reshape(width, channels)
+        proj[w] = jnp.dot(normed[set_rows(r), :], weight, preferred_element_type=F32).astype(BF16)
+
+    def convolve():
         taps = taps_ref[:, pl.ds(pl.multiple_of(t * channels, 128), channels)]
 
         @pl.loop(0, seqs)
@@ -323,6 +328,7 @@
                 conv = conv + taps[offset : offset + 1, :] * moved
             gated[at, :] = (proj[0, at, :].astype(F32) * conv).astype(BF16)
 
+    def mix(r):
         @pl.loop(0, n)
         def _(b):
             at = pl.ds(pl.multiple_of(b * block, 128), block)
@@ -379,15 +385,11 @@
         k = lax.rem(owner // 2 - t // 2 + chips, chips)
         return start, owner, slot, k, lax.rem(owner, 2) == core
 
-    def down_product(b, offset, size):
-        at_cols = pl.ds(pl.multiple_of(b * wide + offset, 128), size)
-
-        @pl.loop(0, 2)
-        def _(turn):
-            r = 1 - turn
-            at = pl.ds(pl.multiple_of(r * rows, rows), rows)
-            weight = full[DOWN][b, :, pl.ds(offset, size)]
-            part[at, at_cols] = jnp.dot(hidden[at, :], weight, preferred_element_type=F32).astype(BF16)
+    def down_product(b, r, offset, size):
+        weight = full[DOWN][b, :, pl.ds(offset, size)]
+        part[set_rows(r), pl.ds(pl.multiple_of(b * wide + offset, 128), size)] = jnp.dot(
+            hidden[set_rows(r), :], weight, preferred_element_type=F32
+        ).astype(BF16)
 
     def to_lane(b, c):
         start, owner, slot, k, lane = place(b, c)
@@ -460,46 +462,46 @@
                 if r == 1:
                     pl.when(has_guest)(lambda: back_copy(slot, guest).start())
 
-    def square_copy(r, k, peer):
-        return pltpu.make_async_remote_copy(
-            src_ref=sq_send.at[r], dst_ref=sq_recv.at[r, k - 1], send_sem=sq_ss.at[r, k - 1],
-            recv_sem=sq_rs.at[r, k - 1], device_id={"tp": peer}, device_id_type=MESH,
-        )
-
-    def squares_send(r):
+    guest = lax.select(f == 1, 0, n - 1)
+
+    def ahead_of(k):
+        return lax.rem(t + k, n_tp)
+
+    def square_copy(k, peer):
+        return pltpu.make_async_remote_copy(
+            src_ref=sq_send.at[0], dst_ref=sq_recv.at[0, k], send_sem=sq_ss.at[0, k],
+            recv_sem=sq_rs.at[0, k], device_id={"tp": peer}, device_id_type=MESH,
+        )
+
+    def edge_squares(k, peer):
+        return pltpu.make_async_remote_copy(
+            src_ref=sq_send.at[1], dst_ref=sq_recv.at[1, k], send_sem=sq_ss.at[1, k],
+            recv_sem=sq_rs.at[1, k], device_id={"fs": guest, "tp": peer}, device_id_type=MESH,
+        )
+
+    def squares_of(r):
         @pl.loop(0, seqs)
         def _(i):
             at = pl.ds(pl.multiple_of(r * rows + i * length, length), length)
             squares = jnp.sum(sq_acc[at, :], axis=1, keepdims=True)
             sq_send[r, i] = jnp.transpose(jnp.broadcast_to(squares, (length, length)))[:8, :]
 
+    def squares_total():
+        total = sq_send[0]
         for k in range(1, n_tp):
-            square_copy(r, k, lax.rem(t + k, n_tp)).start()
-
-    def squares_total(r):
-        for k in range(1, n_tp):
-            square_copy(r, k, lax.rem(t + n_tp - k, n_tp)).wait_recv()
-        total = sq_send[r]
-        for k in range(1, n_tp):
-            total = total + sq_recv[r, k - 1]
+            square_copy(k, t).wait_recv()
+            total = total + sq_recv[0, k]
         return total
 
-    def close(values, squares_of):
+    def close(values, squares):
         gain = out_gain[:, own_columns(t)]
 
         @pl.loop(0, seqs)
         def _(i):
-            factor = column(lax.rsqrt(squares_of[i][:1, :] / width + 1e-06))
+            factor = column(lax.rsqrt(squares[i][:1, :] / width + 1e-06))
             inside = pl.ds(pl.multiple_of(i * length, length), length)
             out_ref[inside, :] = (values[inside, :].astype(F32) * factor * gain).astype(BF16)
 
-    def squares_back(device):
-        return pltpu.make_async_remote_copy(
-            src_ref=sq_back, dst_ref=sq_back, send_sem=guest_sem.at[2], recv_sem=guest_sem.at[3],
-            device_id={"fs": device}, device_id_type=MESH,
-        )
-
-    guest = lax.select(f == 1, 0, n - 1)
     has_guest = (f == 1) | (f == n - 2)
     inward = lax.select(f == 0, 1, n - 2)
 
@@ -511,10 +513,13 @@
 
     @pl.when(jnp.logical_not(is_host))
     def _():
+        small_copy(3).start()
+        small_copy(3).wait()
         order = [("own", w, 0) for w in range(MIXER)] + [("tokens", 0, 0)]
         order += [("other", w, 0) for w in range(MIXER) if direct(w)]
-        for c in range(counts[GATE]):
-            order += [("own", GATE, c), ("own", UP, c), ("other", GATE, c), ("other", UP, c)]
+        for c in range(counts[GATE] + 1):
+            order += [("own", w, c) for w in (GATE, UP) if c < counts[GATE]]
+            order += [("other", w, c - 1) for w in (GATE, UP) if c > 0]
         for kind in ("own", "other"):
             order += [(kind, DOWN, c) for c in range(pieces)]
         for kind, w, c in order:
@@ -533,8 +538,10 @@
                     y_sent(w, f, k)
         for slot in range(columns // piece):
             back_copy(slot, inward).wait_recv()
-        squares_back(inward).wait_recv()
-        close(returned, sq_back)
+        for k in range(n_tp):
+            edge_squares(k, t).wait_recv()
+        sq_total[...] = sum(sq_recv[1, k] for k in range(1, n_tp)) + sq_recv[1, 0]
+        close(returned, sq_total)
 
     @pl.when(is_host)
     def _():
@@ -542,10 +549,14 @@
         own_tokens.start()
         for w in range(MIXER):
             start_own(w, 0)
+        for i in range(4):
+            small_copy(i).start()
         for w in range(7):
             own_copy(w).start()
         own_tokens.wait()
         gather_send(tok_full, 0, 0)
+        for i in range(4):
+            small_copy(i).wait()
         sq_acc[...] = jnp.zeros_like(sq_acc)
         for w in range(MIXER):
             from_inner(w, 0)
@@ -620,20 +631,28 @@
 
         gather_send(tok_full, 0, 1)
         inner_pair(0)
+        for w in range(3):
+            own_copy(w).wait()
+            finish_all(w, 0)
+            project(w, 0)
         outer_pair(0)
         start_pair(2)
-        for w in range(MIXER):
-            own_copy(w).wait()
-            finish_all(w, 0)
-        mixer(0)
+        start_down(0, 1)
+        convolve()
+        own_copy(3).wait()
+        finish_all(3, 0)
+        mix(0)
         sum_send(0)
+        gather_relay(tok_full, 0, 1)
         inner_pair(1)
-        gather_relay(tok_full, 0, 1)
+        gather_finish(tok_full, 0, 1)
         sum_relay(0)
-        gather_finish(tok_full, 0, 1)
         norm_rows(tok_full, mix_gain, 1)
         far_pair(0)
-        mixer(1)
+        for w in range(3):
+            project(w, 1)
+        convolve()
+        mix(1)
         sum_send(1)
         outer_pair(1)
         start_pair(3)
@@ -641,55 +660,54 @@
         inner_pair(2)
         first_rows(0)
         gather_send(first_full, 2, 0)
-        far_pair(1)
         outer_pair(2)
         start_pair(4)
+        inner_down(0)
+        far_pair(1)
         inner_pair(3)
+        outer_pair(3)
+        start_pair(5)
+        start_down(1, 2)
         first_rows(1)
         gather_send(first_full, 2, 1)
         far_pair(2)
-        outer_pair(3)
-        start_pair(5)
+        gather_relay(first_full, 2, 0)
+        outer_pair(4)
         inner_pair(4)
         for w in (GATE, UP):
             own_copy(w).wait()
-        gather_relay(first_full, 2, 0)
-        far_pair(3)
         gather_finish(first_full, 2, 0)
         norm_rows(first_full, ffn_gain, 0)
-        outer_pair(4)
-        start_down(0, 2)
+        far_pair(3)
+        tile(0, 0)
+        outer_pair(5)
+        start_down(2, pieces)
         inner_pair(5)
-        tile(0, 0)
+        inner_down(1)
         tile(1, 0)
         tile(2, 0)
         gather_relay(first_full, 2, 1)
         far_pair(4)
-        outer_pair(5)
-        start_down(2, pieces)
         gather_finish(first_full, 2, 1)
         norm_rows(first_full, ffn_gain, 1)
+        far_pair(5)
+        tile(3, 0)
         for r in range(2):
             for k in range(chips):
                 to_pair(r, k).wait_send()
             for k in range(1, chips):
                 to_far(r, k).wait_send()
-        tile(3, 0)
-        inner_down(0)
-        far_pair(5)
         tile(0, 1)
+        tile(1, 1)
+        tile(2, 1)
         outer_down(0)
-        tile(1, 1)
-        inner_down(1)
-        tile(2, 1)
-        outer_down(1)
         tile(3, 1)
         inner_down(2)
         tile(4, 0)
         tile(4, 1)
-        outer_down(2)
+        outer_down(1)
+        tile(5, 0)
         inner_down(3)
-        tile(5, 0)
         tile(5, 1)
         for c in range(6, last + 1):
             start_pair(c)
@@ -698,35 +716,45 @@
             far_pair(c)
             tile(c, 0)
             tile(c, 1)
-        for c in range(4, pieces):
-            inner_down(c)
         own_copy(DOWN).wait()
-        near = f + inner
-        down_product(f, 0, wide)
-        for c in range(pieces):
-            to_lane(f, c)
+        near, outer = f + inner, f - inner
+        batch = 2 if pieces % 2 == 0 else 1
+
+        def produce(b, first, count):
+            for r in (1, 0):
+                down_product(b, r, pl.multiple_of(first * piece, 128), count * piece)
+            for i in range(count):
+                to_lane(b, first + i)
+
+        def far_down(c):
+            if c < pieces:
+                from_far(DOWN, c)
+
+        def near_pieces(first, count):
+            for c in range(first, first + count):
+                finish(DOWN, c, near)
+            produce(near, first, count)
+
+        near_pieces(0, batch)
+        outer_down(2)
+        produce(f, 0, pieces)
+        far_down(0)
+        for c in range(batch):
+            combine(near, c)
         for c in range(3, pieces):
             outer_down(c)
-        from_far(DOWN, 0)
-        for c in range(pieces):
-            finish(DOWN, c, near)
-        down_product(near, 0, wide)
-        for c in range(pieces):
-            to_lane(near, c)
-        for c in range(1, min(2, pieces)):
-            from_far(DOWN, c)
         for c in range(pieces):
             combine(f, c)
-        for c in range(2, min(3, pieces)):
-            from_far(DOWN, c)
-        for c in range(pieces):
+        for first in range(batch, pieces, batch):
+            near_pieces(first, batch)
+        far_down(1)
+        for c in range(batch, pieces):
             combine(near, c)
+        far_down(2)
         drain(range(DOWN))
         for r in range(2):
             gather_sent(tok_full, 0, r)
             gather_sent(first_full, 2, r)
-        for c in range(3, pieces):
-            from_far(DOWN, c)
 
         def others(visit):
             @pl.loop(1, n - 2)
@@ -735,53 +763,62 @@
                     b = f + toward * (1 + s)
                     pl.when((b >= 0) & (b < n))(lambda: visit(b))
 
-        outer = f - inner
-
-        def take(b, c):
-            finish(DOWN, c, b)
-            down_product(b, pl.multiple_of(c * piece, 128), piece)
-            to_lane(b, c)
+        def take(b, first, count):
+            for c in range(first, first + count):
+                finish(DOWN, c, b)
+            produce(b, first, count)
+
+        def join(b, first, count):
+            for c in range(first, first + count):
+                combine(b, c)
+
+        def settle_range(first, end):
+            @pl.loop(first, end)
+            def _(i):
+                settle(f, i)
+                settle(near, i)
+
+        batches = [(0, batch)] + [(c, 1) for c in range(batch, pieces)]
+        for first, count in batches:
+            take(outer, first, count)
+            for c in range(max(first + count, 3), pieces if first == 0 else 0):
+                from_far(DOWN, c)
+            if first + count == pieces:
+                settle_range(pieces // 2, pieces)
+            elif first > 0:
+                settle_range(0, pieces // 2)
+            others(lambda b: take(b, first, count))
+
+            join(outer, first, count)
+            others(lambda b: join(b, first, count))
 
         @pl.loop(0, pieces)
         def _(c):
-            others(lambda b: take(b, c))
-            take(outer, c)
-            others(lambda b: combine(b, c))
-            combine(outer, c)
-
-            @pl.when(c >= LAG)
-            def _():
-                others(lambda b: settle(b, c - LAG))
-                settle(outer, c - LAG)
-
-        @pl.loop(0, pieces)
-        def _(i):
-            settle(f, i)
-            settle(near, i)
-
-        for c in range(max(pieces - LAG, 0), pieces):
             others(lambda b: settle(b, c))
             settle(outer, c)
 
-        squares_send(1)
-        squares_send(0)
-        sq_back[...] = squares_total(1)
+        squares_of(1)
 
         @pl.when(has_guest)
         def _():
-            squares_back(guest).start()
-
-        sq_total[...] = squares_total(0)
+            for k in range(n_tp):
+                edge_squares(k, ahead_of(k)).start()
+
+        squares_of(0)
+        for k in range(1, n_tp):
+            square_copy(k, ahead_of(k)).start()
+        sq_total[...] = squares_total()
         close(second_own, sq_total)
 
         @pl.when(has_guest)
         def _():
-            squares_back(guest).wait_send()
+            for k in range(n_tp):
+                edge_squares(k, ahead_of(k)).wait_send()
             back_sent()
 
+        for k in range(1, n_tp):
+            square_copy(k, ahead_of(k)).wait_send()
         for r in range(2):
-            for k in range(1, n_tp):
-                square_copy(r, k, lax.rem(t + k, n_tp)).wait_send()
             for k in range(chips):
                 down_sent(r, k)
         drain((DOWN,))
@@ -800,7 +837,7 @@
         spans[DOWN] = tuple((start, piece) for start in range(0, down.shape[1], piece))
         slots = sum(len(tiles) for tiles in spans)
         channels, units = outer.shape[1], gate.shape[1]
-        others, y_others = max(n_tp - 1, 1), max(parts - 1, 1)
+        y_others = max(parts - 1, 1)
         per_owner = columns // piece
         dma = pltpu.SemaphoreType.DMA
         scratch = [pltpu.VMEM((n,) + a.shape, BF16) for a in weights]
@@ -819,20 +856,20 @@
             pltpu.VMEM((rows, columns), F32),
             pltpu.VMEM((2 * rows, 128), F32),
             pltpu.VMEM((2, seqs, 8, length), F32),
-            pltpu.VMEM((2, others, seqs, 8, length), F32),
+            pltpu.VMEM((2, n_tp, seqs, 8, length), F32),
             pltpu.VMEM((seqs, 8, length), F32),
-            pltpu.VMEM((seqs, 8, length), F32),
+            pltpu.VMEM((1, width), F32), pltpu.VMEM(taps.shape, F32),
+            pltpu.VMEM((1, width), F32), pltpu.VMEM((1, width), F32),
             dma((7, n + 1)), dma((slots, n)),
             dma((7, n, y_others)), dma((slots, n, y_others)),
-            dma((8,)), dma((3, 2, chips)), dma((3, 2, chips)), dma((3, 2, chips)), dma((3, 2, chips)),
+            dma((12,)), dma((3, 2, chips)), dma((3, 2, chips)), dma((3, 2, chips)), dma((3, 2, chips)),
             dma((2, chips)), dma((2, chips, per_owner)), dma((2, chips)), dma((2, chips, per_owner)),
-            dma((2, others)), dma((2, others)), dma((1,)), dma((per_owner,)), dma((4,)),
+            dma((2, n_tp)), dma((2, n_tp)), dma((1,)), dma((per_owner,)), dma((2,)),
         ]
-        hbm, vmem = pl.BlockSpec(memory_space=pl.ANY), pl.BlockSpec(memory_space=pltpu.VMEM)
         out = pl.pallas_call(
             functools.partial(kernel, n, parts, n_tp, length, tuple(spans)),
             out_shape=jax.ShapeDtypeStruct((rows, columns), BF16),
-            in_specs=[hbm, vmem, hbm, hbm, hbm, vmem, hbm, vmem, hbm, hbm, hbm, vmem],
+            in_specs=[pl.BlockSpec(memory_space=pl.ANY)] * 12,
             out_specs=pl.BlockSpec(memory_space=pltpu.VMEM),
             scratch_shapes=scratch,
             compiler_params=pltpu.CompilerParams(

time: 163 us -> 153 us (0.939)
  Pallas kernels: 161 us -> 151 us
    pallas_call x1, Pallas kernels: 161 us -> 151 us  [local(): pl.pallas_call(functools.partial(kernel, n, parts, n_tp, length, tuple(sp...]
where the time goes in v2:
time: 153 us
  Pallas kernels  151 us (99%)
  local copies, waits for them, and re-layouts  1.87 us (1%)
    pallas_call x1, Pallas kernels, local(): pl.pallas_call(functools.partial(kernel, n, parts, n_tp, length, tuple(sp...  151 us

profile of v2, /device:TPU:0, one launch (start us, length us, event | category | flops | bytes accessed | tf_op | source)
XLA Modules:
  0.0 153.1 jit_solution(8600720644763891711)
XLA Ops:
  0.0 151.2 %shard_map.118 = bf16[512,512]{1,0:T(8,128)(2,1)} custom-call(bf16[512,512]{1,0:T(8,128)(2,1)} %bitcast.6, f32[1,2048]{1,0:T(1,128)} %bitcast.7, bf16[512,256]{1,0:T(8,128)(2,1)} %w0.1, bf16[512,256]{1,0:T(8,128)(2,1)} %w1.1, bf16[512,256]{1,0:T(8,128)(2,1)} %w2.1, f32[3,1024]{1,0:T(4,128)} %taps_in.1, bf16[256,512]{1,0:T(8,128)(2,1)} %w3.1, ...), custom_call_target="tpu_custom_call" | custom-call | tf_op jit(solution)/shard_map/pallas_call | solution.py:869
  151.2 1.9 %copy.14 = bf16[4,128,512]{2,1,0:T(8,128)(2,1)} copy(bf16[4,128,512]{2,1,0:T(8,128)(2,1)} %bitcast.5) | data formatting | bytes 1048576

commit v3 on v2

--- a/solution.py
+++ b/solution.py
@@ -13,6 +13,7 @@
 MIXER = 4
 GATE, UP, DOWN = 4, 5, 6
 SHARED = 1
+TRAIL = 2
 LAG = 2
 
 
@@ -22,29 +23,30 @@
     return tuple((start, min(256, units - start)) for start in range(0, units, 256))
 
 
-def column(rows):
-    wide = jnp.broadcast_to(rows, (rows.shape[1], rows.shape[1]))
-    return jnp.transpose(wide)[:, :1]
+def spread(rows):
+    return jnp.transpose(jnp.broadcast_to(rows, (rows.shape[1], rows.shape[1])))
 
 
 def kernel(
     n, parts, n_tp, length, spans,
     tok_ref, mix_gain_in, w0, w1, w2, taps_in, w3, ffn_gain_in, w4, w5, w6, out_gain_in,
     out_ref,
-    f0, f1, f2, f3, f4, f5, f6,
+    f0, f1, f2, f3, pair_full, f6,
     tok_full, normed, proj, gated, part, pair_recv, far_recv, first_full, hidden, returned, second_own, sq_acc,
     sq_send, sq_recv, sq_total, mix_gain, taps_ref, ffn_gain, out_gain,
     z_send, z_recv, y_send, y_recv, own_sem, pair_ss, pair_rs, far_ss, far_rs,
     down_pair_ss, down_pair_rs, down_far_ss, down_far_rs, sq_ss, sq_rs, back_ss, back_rs, guest_sem,
 ):
     own = (w0, w1, w2, w3, w4, w5, w6)
-    full = (f0, f1, f2, f3, f4, f5, f6)
+    full = (f0, f1, f2, f3, pair_full.at[0], pair_full.at[1], f6)
     f, g, t = lax.axis_index("fs"), lax.axis_index("grp"), lax.axis_index("tp")
     rows, columns = tok_ref.shape
     width = columns * n_tp
     seqs = rows // length
     counts = [len(tiles) for tiles in spans]
-    bases = [sum(counts[:w]) for w in range(7)]
+    groups = (0, 1, 2, 3, GATE, DOWN)
+    ranks = {w: i for i, w in enumerate(groups)}
+    bases = {w: sum(counts[v] for v in groups[:i]) for w, i in ranks.items()}
 
     def y_peer(k):
         return lax.rem(g + k, parts)
@@ -61,13 +63,41 @@
             at = pl.ds(pl.multiple_of(c * width_c, 128), width_c)
         return pl.ds(pl.multiple_of(half * size, 8), size), at
 
+    def members(w):
+        return (GATE, UP) if w == GATE else (w,)
+
     def region(w, blk, half, c):
         at_rows, at_cols = span(w, half, c)
+        if w == GATE:
+            return pair_full.at[:, blk, at_rows, at_cols]
         return full[w].at[blk, at_rows, at_cols]
+
+    def landing(v, blk, half, c):
+        at_rows, at_cols = span(v, half, c)
+        if v in (GATE, UP):
+            return pair_full.at[v - GATE, blk, at_rows, at_cols]
+        return full[v].at[blk, at_rows, at_cols]
 
     def piece_of(w, half, c):
         at_rows, at_cols = span(w, half, c)
         return own[w].at[at_rows, at_cols]
+
+    def small_copy(i):
+        pairs = ((mix_gain_in, mix_gain), (taps_in, taps_ref), (ffn_gain_in, ffn_gain), (out_gain_in, out_gain))
+        return pltpu.make_async_copy(*pairs[i], own_sem.at[8 + i])
+
+    def own_tokens():
+        mine = tok_full.at[pl.ds(0, rows), pl.ds(pl.multiple_of(t * columns, 128), columns)]
+        return pltpu.make_async_copy(tok_ref, mine, own_sem.at[7])
+
+    hosting = (f >= 1) & (f <= n - 2)
+    small_copy(3).start()
+
+    @pl.when(hosting)
+    def _():
+        own_tokens().start()
+        for i in range(3):
+            small_copy(i).start()
 
     barrier = pltpu.get_barrier_semaphore()
     for k in range(1, n_tp):
@@ -91,33 +121,39 @@
 
     def half_block(w, blk):
         size = own[w].shape[0] // parts
-        return full[w].at[blk, pl.ds(pl.multiple_of(g * size, 8), size), :]
+        at_rows = pl.ds(pl.multiple_of(g * size, 8), size)
+        if w == GATE:
+            return pair_full.at[:, blk, at_rows, :]
+        return full[w].at[blk, at_rows, :]
 
     def z_sent(w, blk, step):
         half = half_block(w, blk)
         pltpu.make_async_remote_copy(
-            src_ref=half, dst_ref=half, send_sem=z_send.at[w, z_slot(blk, step)], recv_sem=z_recv.at[bases[w], blk],
+            src_ref=half, dst_ref=half, send_sem=z_send.at[ranks[w], z_slot(blk, step)], recv_sem=z_recv.at[bases[w], 0],
             device_id={"fs": f + step}, device_id_type=MESH,
         ).wait_send()
 
     def y_sent(w, blk, k):
         half = half_block(w, blk)
         pltpu.make_async_remote_copy(
-            src_ref=half, dst_ref=half, send_sem=y_send.at[w, blk, k - 1], recv_sem=y_recv.at[bases[w], blk, k - 1],
+            src_ref=half, dst_ref=half, send_sem=y_send.at[ranks[w], blk, k - 1], recv_sem=y_recv.at[bases[w], 0, k - 1],
             device_id={"grp": y_peer(k)}, device_id_type=MESH,
         ).wait_send()
 
-    def z_copy(w, c, blk, src, step):
+    def seat(blk, host):
+        return blk - lax.select(blk > host, 1, 0)
+
+    def z_copy(w, c, blk, src, dst, step, host):
         return pltpu.make_async_remote_copy(
-            src_ref=src, dst_ref=region(w, blk, g, c),
-            send_sem=z_send.at[w, z_slot(blk, step)], recv_sem=z_recv.at[bases[w] + c, blk],
+            src_ref=src, dst_ref=dst, send_sem=z_send.at[ranks[w], z_slot(blk, step)],
+            recv_sem=z_recv.at[bases[w] + c, seat(blk, host)],
             device_id={"fs": f + step}, device_id_type=MESH,
         )
 
     def y_copy(w, c, blk, half, k, peer):
         return pltpu.make_async_remote_copy(
             src_ref=region(w, blk, half, c), dst_ref=region(w, blk, half, c),
-            send_sem=y_send.at[w, blk, k - 1], recv_sem=y_recv.at[bases[w] + c, blk, k - 1],
+            send_sem=y_send.at[ranks[w], blk, k - 1], recv_sem=y_recv.at[bases[w] + c, seat(blk, f), k - 1],
             device_id={"grp": peer}, device_id_type=MESH,
         )
 
@@ -126,24 +162,24 @@
     inner = lax.select(2 * f + 1 < n, 1, -1)
 
     def start_own(w, c):
-        src = piece_of(w, g, c)
-
-        @pl.when(f + 1 <= last_host)
-        def _():
-            z_copy(w, c, f, src, 1).start()
-
-        @pl.when(f - 1 >= first_host)
-        def _():
-            z_copy(w, c, f, src, -1).start()
-
-    def other_half(w, c, k):
-        half = lax.rem(g + parts - k, parts)
+        def towards(step):
+            for v in members(w):
+                z_copy(w, c, f, piece_of(v, g, c), landing(v, f, g, c), step, f + step).start()
+
+        pl.when(f + 1 <= last_host)(lambda: towards(1))
+        pl.when(f - 1 >= first_host)(lambda: towards(-1))
+
+    def start_other(w, c):
         inward = lax.select(f == 0, 1, n - 2)
-        return pltpu.make_async_remote_copy(
-            src_ref=piece_of(w, half, c), dst_ref=region(w, f, half, c),
-            send_sem=y_send.at[w, f, k - 1], recv_sem=y_recv.at[bases[w] + c, f, k - 1],
-            device_id={"fs": inward}, device_id_type=MESH,
-        )
+        for k in range(1, parts):
+            half = lax.rem(g + parts - k, parts)
+            for v in members(w):
+                pltpu.make_async_remote_copy(
+                    src_ref=piece_of(v, half, c), dst_ref=landing(v, f, half, c),
+                    send_sem=y_send.at[ranks[w], f, k - 1],
+                    recv_sem=y_recv.at[bases[w] + c, seat(f, inward), k - 1],
+                    device_id={"fs": inward}, device_id_type=MESH,
+                ).start()
 
     def direct(w):
         return w >= SHARED
@@ -154,14 +190,15 @@
 
         @pl.when((blk >= 0) & (blk < n))
         def _():
-            z_copy(w, c, blk, region(w, blk, g, c), step).wait_recv()
+            here = region(w, blk, g, c)
+            z_copy(w, c, blk, here, here, step, f).wait_recv()
 
             def share():
                 for k in range(1, parts):
                     y_copy(w, c, blk, g, k, y_peer(k)).start()
 
             def onward():
-                z_copy(w, c, blk, region(w, blk, g, c), step).start()
+                z_copy(w, c, blk, here, here, step, f + step).start()
 
             pl.when((f + step <= last_host) & (f + step >= first_host))(onward)
             if next_to_edge and direct(w):
@@ -193,10 +230,6 @@
 
     def own_copy(w):
         return pltpu.make_async_copy(own[w], full[w].at[f], own_sem.at[w])
-
-    def small_copy(i):
-        pairs = ((mix_gain_in, mix_gain), (taps_in, taps_ref), (ffn_gain_in, ffn_gain), (out_gain_in, out_gain))
-        return pltpu.make_async_copy(*pairs[i], own_sem.at[8 + i])
 
     def own_columns(owner):
         return pl.ds(pl.multiple_of(owner * columns, 128), columns)
@@ -480,11 +513,10 @@
         )
 
     def squares_of(r):
-        @pl.loop(0, seqs)
-        def _(i):
-            at = pl.ds(pl.multiple_of(r * rows + i * length, length), length)
-            squares = jnp.sum(sq_acc[at, :], axis=1, keepdims=True)
-            sq_send[r, i] = jnp.transpose(jnp.broadcast_to(squares, (length, length)))[:8, :]
+        for i in range(seqs):
+            at = pl.ds(r * rows + i * length, length)
+            sums = jnp.sum(jnp.transpose(sq_acc[at, :]), axis=0, keepdims=True)
+            sq_send[r, i] = jnp.broadcast_to(sums, (8, length))
 
     def squares_total():
         total = sq_send[0]
@@ -495,12 +527,13 @@
 
     def close(values, squares):
         gain = out_gain[:, own_columns(t)]
-
-        @pl.loop(0, seqs)
-        def _(i):
-            factor = column(lax.rsqrt(squares[i][:1, :] / width + 1e-06))
-            inside = pl.ds(pl.multiple_of(i * length, length), length)
-            out_ref[inside, :] = (values[inside, :].astype(F32) * factor * gain).astype(BF16)
+        for i in range(seqs):
+            factor = spread(lax.rsqrt(squares[i][:1, :] / width + 1e-06))
+            inside = pl.ds(i * length, length)
+            for start in range(0, columns, length):
+                at = pl.ds(start, min(length, columns - start))
+                scaled = values[inside, at].astype(F32) * factor[:, : at.size] * gain[:, start : start + at.size]
+                out_ref[inside, at] = scaled.astype(BF16)
 
     has_guest = (f == 1) | (f == n - 2)
     inward = lax.select(f == 0, 1, n - 2)
@@ -513,13 +546,12 @@
 
     @pl.when(jnp.logical_not(is_host))
     def _():
-        small_copy(3).start()
         small_copy(3).wait()
         order = [("own", w, 0) for w in range(MIXER)] + [("tokens", 0, 0)]
         order += [("other", w, 0) for w in range(MIXER) if direct(w)]
-        for c in range(counts[GATE] + 1):
-            order += [("own", w, c) for w in (GATE, UP) if c < counts[GATE]]
-            order += [("other", w, c - 1) for w in (GATE, UP) if c > 0]
+        for c in range(counts[GATE] + TRAIL):
+            order += [("own", GATE, c)] if c < counts[GATE] else []
+            order += [("other", GATE, c - TRAIL)] if c >= TRAIL else []
         for kind in ("own", "other"):
             order += [(kind, DOWN, c) for c in range(pieces)]
         for kind, w, c in order:
@@ -528,32 +560,33 @@
             elif kind == "tokens":
                 tokens_in(inward).start()
             else:
-                for k in range(1, parts):
-                    other_half(w, c, k).start()
+                start_other(w, c)
         tokens_in(inward).wait_send()
-        for w in range(7):
+        for w in groups:
             z_sent(w, f, lax.select(f == 0, 1, -1))
             if direct(w):
                 for k in range(1, parts):
                     y_sent(w, f, k)
+        def take_back(slot):
+            back_copy(slot, inward).wait_recv()
+
+        def take_squares(k):
+            edge_squares(k, t).wait_recv()
+
         for slot in range(columns // piece):
-            back_copy(slot, inward).wait_recv()
+            take_back(slot)
         for k in range(n_tp):
-            edge_squares(k, t).wait_recv()
+            take_squares(k)
         sq_total[...] = sum(sq_recv[1, k] for k in range(1, n_tp)) + sq_recv[1, 0]
         close(returned, sq_total)
 
     @pl.when(is_host)
     def _():
-        own_tokens = pltpu.make_async_copy(tok_ref, block_of(tok_full, 0, t), own_sem.at[7])
-        own_tokens.start()
         for w in range(MIXER):
             start_own(w, 0)
-        for i in range(4):
-            small_copy(i).start()
         for w in range(7):
             own_copy(w).start()
-        own_tokens.wait()
+        own_tokens().wait()
         gather_send(tok_full, 0, 0)
         for i in range(4):
             small_copy(i).wait()
@@ -566,22 +599,18 @@
         def start_pair(c):
             if c <= last:
                 start_own(GATE, c)
-                start_own(UP, c)
 
         def inner_pair(c):
             if c <= last:
                 from_inner(GATE, c)
-                from_inner(UP, c)
 
         def outer_pair(c):
             if c <= last:
                 from_outer(GATE, c)
-                from_outer(UP, c)
 
         def far_pair(c):
             if c <= last:
                 from_far(GATE, c)
-                from_far(UP, c)
 
         def start_down(first, end):
             for c in range(first, min(end, pieces)):
@@ -598,8 +627,7 @@
         def tile(c, r):
             if c <= last:
                 if r == 0:
-                    for w in (GATE, UP):
-                        finish_all(w, c)
+                    finish_all(GATE, c)
                 hidden_tiles(c, r)
 
         def drain(group):
@@ -618,6 +646,7 @@
 
         start_pair(0)
         start_pair(1)
+        start_pair(2)
         gather_relay(tok_full, 0, 0)
         from_far(0, 0)
         gather_finish(tok_full, 0, 0)
@@ -635,63 +664,61 @@
             own_copy(w).wait()
             finish_all(w, 0)
             project(w, 0)
-        outer_pair(0)
-        start_pair(2)
-        start_down(0, 1)
         convolve()
         own_copy(3).wait()
         finish_all(3, 0)
         mix(0)
         sum_send(0)
+        inner_pair(1)
         gather_relay(tok_full, 0, 1)
-        inner_pair(1)
         gather_finish(tok_full, 0, 1)
+        outer_pair(0)
         sum_relay(0)
         norm_rows(tok_full, mix_gain, 1)
-        far_pair(0)
-        for w in range(3):
-            project(w, 1)
+        inner_pair(2)
+        project(0, 1)
+        project(1, 1)
+        outer_pair(1)
+        start_pair(3)
+        project(2, 1)
         convolve()
         mix(1)
         sum_send(1)
-        outer_pair(1)
-        start_pair(3)
+        far_pair(0)
         sum_relay(1)
-        inner_pair(2)
+        outer_pair(2)
+        start_pair(4)
+        far_pair(1)
         first_rows(0)
         gather_send(first_full, 2, 0)
-        outer_pair(2)
-        start_pair(4)
-        inner_down(0)
-        far_pair(1)
         inner_pair(3)
         outer_pair(3)
         start_pair(5)
-        start_down(1, 2)
+        far_pair(2)
         first_rows(1)
         gather_send(first_full, 2, 1)
-        far_pair(2)
-        gather_relay(first_full, 2, 0)
+        inner_pair(4)
         outer_pair(4)
-        inner_pair(4)
+        start_down(0, 1)
+        far_pair(3)
         for w in (GATE, UP):
             own_copy(w).wait()
+        gather_relay(first_full, 2, 0)
+        inner_pair(5)
         gather_finish(first_full, 2, 0)
+        outer_pair(5)
+        start_down(1, pieces)
         norm_rows(first_full, ffn_gain, 0)
-        far_pair(3)
+        far_pair(4)
         tile(0, 0)
-        outer_pair(5)
-        start_down(2, pieces)
-        inner_pair(5)
-        inner_down(1)
         tile(1, 0)
+        far_pair(5)
         tile(2, 0)
         gather_relay(first_full, 2, 1)
-        far_pair(4)
+        tile(3, 0)
+        inner_down(0)
         gather_finish(first_full, 2, 1)
         norm_rows(first_full, ffn_gain, 1)
-        far_pair(5)
-        tile(3, 0)
         for r in range(2):
             for k in range(chips):
                 to_pair(r, k).wait_send()
@@ -699,15 +726,16 @@
                 to_far(r, k).wait_send()
         tile(0, 1)
         tile(1, 1)
+        inner_down(1)
         tile(2, 1)
-        outer_down(0)
         tile(3, 1)
         inner_down(2)
         tile(4, 0)
+        outer_down(0)
         tile(4, 1)
-        outer_down(1)
         tile(5, 0)
         inner_down(3)
+        outer_down(1)
         tile(5, 1)
         for c in range(6, last + 1):
             start_pair(c)
@@ -730,28 +758,31 @@
             if c < pieces:
                 from_far(DOWN, c)
 
+        def join(b, first, count):
+            for c in range(first, first + count):
+                combine(b, c)
+
         def near_pieces(first, count):
             for c in range(first, first + count):
                 finish(DOWN, c, near)
             produce(near, first, count)
 
+        produce(f, 0, batch)
         near_pieces(0, batch)
         outer_down(2)
-        produce(f, 0, pieces)
+        join(f, 0, batch)
+        join(near, 0, batch)
         far_down(0)
-        for c in range(batch):
-            combine(near, c)
+        for first in range(batch, pieces, batch):
+            produce(f, first, batch)
+            near_pieces(first, batch)
+            join(f, first, batch)
+            join(near, first, batch)
+        far_down(1)
         for c in range(3, pieces):
             outer_down(c)
-        for c in range(pieces):
-            combine(f, c)
-        for first in range(batch, pieces, batch):
-            near_pieces(first, batch)
-        far_down(1)
-        for c in range(batch, pieces):
-            combine(near, c)
         far_down(2)
-        drain(range(DOWN))
+        drain(groups[:-1])
         for r in range(2):
             gather_sent(tok_full, 0, r)
             gather_sent(first_full, 2, r)
@@ -768,34 +799,45 @@
                 finish(DOWN, c, b)
             produce(b, first, count)
 
-        def join(b, first, count):
-            for c in range(first, first + count):
-                combine(b, c)
-
         def settle_range(first, end):
             @pl.loop(first, end)
             def _(i):
                 settle(f, i)
                 settle(near, i)
 
-        batches = [(0, batch)] + [(c, 1) for c in range(batch, pieces)]
-        for first, count in batches:
-            take(outer, first, count)
-            for c in range(max(first + count, 3), pieces if first == 0 else 0):
-                from_far(DOWN, c)
-            if first + count == pieces:
-                settle_range(pieces // 2, pieces)
-            elif first > 0:
-                settle_range(0, pieces // 2)
-            others(lambda b: take(b, first, count))
-
-            join(outer, first, count)
-            others(lambda b: join(b, first, count))
-
-        @pl.loop(0, pieces)
-        def _(c):
+        def far_take(c):
+            others(lambda b: take(b, c, 1))
+
+        def far_join(c):
+            others(lambda b: combine(b, c))
+
+        far_take(0)
+        far_join(0)
+        take(outer, 0, batch)
+        for c in range(3, pieces):
+            from_far(DOWN, c)
+        for c in range(1, batch):
+            far_take(c)
+        join(outer, 0, batch)
+        settle_range(0, batch)
+        for c in range(1, batch):
+            far_join(c)
+        for c in range(batch, pieces):
+            take(outer, c, 1)
+            if c > batch:
+                far_join(c - 1)
+            join(outer, c, 1)
+            if c == batch:
+                settle_range(batch, pieces)
+            far_take(c)
+        if pieces > batch:
+            far_join(pieces - 1)
+            for c in range(batch):
+                settle(outer, c)
+        for c in range(pieces):
             others(lambda b: settle(b, c))
-            settle(outer, c)
+            if c >= batch or pieces == batch:
+                settle(outer, c)
 
         squares_of(1)
 
@@ -835,12 +877,14 @@
         spans = [((0, a.shape[1]),) for a in weights]
         spans[GATE] = spans[UP] = tiles_of(gate.shape[1])
         spans[DOWN] = tuple((start, piece) for start in range(0, down.shape[1], piece))
-        slots = sum(len(tiles) for tiles in spans)
+        slots = sum(len(tiles) for w, tiles in enumerate(spans) if w != UP)
+        groups = len(weights) - 1
         channels, units = outer.shape[1], gate.shape[1]
         y_others = max(parts - 1, 1)
         per_owner = columns // piece
         dma = pltpu.SemaphoreType.DMA
-        scratch = [pltpu.VMEM((n,) + a.shape, BF16) for a in weights]
+        scratch = [pltpu.VMEM((n,) + a.shape, BF16) for a in weights[:GATE]]
+        scratch += [pltpu.VMEM((2, n) + gate.shape, BF16), pltpu.VMEM((n,) + down.shape, BF16)]
         chips = n_tp // 2
         scratch += [
             pltpu.VMEM((2 * rows, width), BF16),
@@ -860,8 +904,8 @@
             pltpu.VMEM((seqs, 8, length), F32),
             pltpu.VMEM((1, width), F32), pltpu.VMEM(taps.shape, F32),
             pltpu.VMEM((1, width), F32), pltpu.VMEM((1, width), F32),
-            dma((7, n + 1)), dma((slots, n)),
-            dma((7, n, y_others)), dma((slots, n, y_others)),
+            dma((groups, n + 1)), dma((slots, n - 1)),
+            dma((groups, n, y_others)), dma((slots, n - 1, y_others)),
             dma((12,)), dma((3, 2, chips)), dma((3, 2, chips)), dma((3, 2, chips)), dma((3, 2, chips)),
             dma((2, chips)), dma((2, chips, per_owner)), dma((2, chips)), dma((2, chips, per_owner)),
             dma((2, n_tp)), dma((2, n_tp)), dma((1,)), dma((per_owner,)), dma((2,)),

time: 153 us -> 148 us (0.967)
  Pallas kernels: 151 us -> 146 us
    pallas_call x1, Pallas kernels: 151 us -> 146 us  [local(): pl.pallas_call(functools.partial(kernel, n, parts, n_tp, length, tuple(sp...]
where the time goes in v3:
time: 148 us
  Pallas kernels  146 us (99%)
  local copies, waits for them, and re-layouts  1.87 us (1%)
    pallas_call x1, Pallas kernels, local(): pl.pallas_call(functools.partial(kernel, n, parts, n_tp, length, tuple(sp...  146 us

profile of v3, /device:TPU:0, one launch (start us, length us, event | category | flops | bytes accessed | tf_op | source)
XLA Modules:
  0.0 147.8 jit_solution(10731235893489232244)
XLA Ops:
  0.0 145.9 %shard_map.118 = bf16[512,512]{1,0:T(8,128)(2,1)} custom-call(bf16[512,512]{1,0:T(8,128)(2,1)} %bitcast.6, f32[1,2048]{1,0:T(1,128)} %bitcast.7, bf16[512,256]{1,0:T(8,128)(2,1)} %w0.1, bf16[512,256]{1,0:T(8,128)(2,1)} %w1.1, bf16[512,256]{1,0:T(8,128)(2,1)} %w2.1, f32[3,1024]{1,0:T(4,128)} %taps_in.1, bf16[256,512]{1,0:T(8,128)(2,1)} %w3.1, ...), custom_call_target="tpu_custom_call" | custom-call | tf_op jit(solution)/shard_map/pallas_call | solution.py:913
  145.9 1.9 %copy.14 = bf16[4,128,512]{2,1,0:T(8,128)(2,1)} copy(bf16[4,128,512]{2,1,0:T(8,128)(2,1)} %bitcast.5) | data formatting | bytes 1048576

commit v4 on v3

--- a/solution.py
+++ b/solution.py
@@ -30,12 +30,12 @@
 def kernel(
     n, parts, n_tp, length, spans,
     tok_ref, mix_gain_in, w0, w1, w2, taps_in, w3, ffn_gain_in, w4, w5, w6, out_gain_in,
-    out_ref,
+    out_hbm,
     f0, f1, f2, f3, pair_full, f6,
     tok_full, normed, proj, gated, part, pair_recv, far_recv, first_full, hidden, returned, second_own, sq_acc,
-    sq_send, sq_recv, sq_total, mix_gain, taps_ref, ffn_gain, out_gain,
+    sq_send, sq_recv, sq_total, out_ref, mix_gain, taps_ref, ffn_gain, out_gain,
     z_send, z_recv, y_send, y_recv, own_sem, pair_ss, pair_rs, far_ss, far_rs,
-    down_pair_ss, down_pair_rs, down_far_ss, down_far_rs, sq_ss, sq_rs, back_ss, back_rs, guest_sem,
+    down_pair_ss, down_pair_rs, down_far_ss, down_far_rs, sq_ss, sq_rs, back_ss, back_rs, guest_sem, out_sem,
 ):
     own = (w0, w1, w2, w3, w4, w5, w6)
     full = (f0, f1, f2, f3, pair_full.at[0], pair_full.at[1], f6)
@@ -516,7 +516,7 @@
         for i in range(seqs):
             at = pl.ds(r * rows + i * length, length)
             sums = jnp.sum(jnp.transpose(sq_acc[at, :]), axis=0, keepdims=True)
-            sq_send[r, i] = jnp.broadcast_to(sums, (8, length))
+            sq_send[r, i : i + 1, :] = sums
 
     def squares_total():
         total = sq_send[0]
@@ -525,15 +525,20 @@
             total = total + sq_recv[0, k]
         return total
 
+    def put_out(i):
+        at = pl.ds(i * length, length)
+        return pltpu.make_async_copy(out_ref.at[at, :], out_hbm.at[at, :], out_sem.at[i])
+
     def close(values, squares):
         gain = out_gain[:, own_columns(t)]
         for i in range(seqs):
-            factor = spread(lax.rsqrt(squares[i][:1, :] / width + 1e-06))
+            factor = spread(lax.rsqrt(squares[i : i + 1, :] / width + 1e-06))
             inside = pl.ds(i * length, length)
             for start in range(0, columns, length):
                 at = pl.ds(start, min(length, columns - start))
                 scaled = values[inside, at].astype(F32) * factor[:, : at.size] * gain[:, start : start + at.size]
                 out_ref[inside, at] = scaled.astype(BF16)
+            put_out(i).start()
 
     has_guest = (f == 1) | (f == n - 2)
     inward = lax.select(f == 0, 1, n - 2)
@@ -547,8 +552,8 @@
     @pl.when(jnp.logical_not(is_host))
     def _():
         small_copy(3).wait()
-        order = [("own", w, 0) for w in range(MIXER)] + [("tokens", 0, 0)]
-        order += [("other", w, 0) for w in range(MIXER) if direct(w)]
+        order = [("own", w, c) for w in range(MIXER) for c in range(counts[w])] + [("tokens", 0, 0)]
+        order += [("other", w, c) for w in range(MIXER) if direct(w) for c in range(counts[w])]
         for c in range(counts[GATE] + TRAIL):
             order += [("own", GATE, c)] if c < counts[GATE] else []
             order += [("other", GATE, c - TRAIL)] if c >= TRAIL else []
@@ -582,8 +587,9 @@
 
     @pl.when(is_host)
     def _():
-        for w in range(MIXER):
-            start_own(w, 0)
+        mixer_tiles = [(w, c) for w in range(MIXER) for c in range(counts[w])]
+        for w, c in mixer_tiles:
+            start_own(w, c)
         for w in range(7):
             own_copy(w).start()
         own_tokens().wait()
@@ -591,9 +597,10 @@
         for i in range(4):
             small_copy(i).wait()
         sq_acc[...] = jnp.zeros_like(sq_acc)
-        for w in range(MIXER):
-            from_inner(w, 0)
-            from_outer(w, 0)
+        sq_send[...] = jnp.zeros_like(sq_send)
+        for w, c in mixer_tiles:
+            from_inner(w, c)
+            from_outer(w, c)
         last = counts[GATE] - 1
 
         def start_pair(c):
@@ -648,11 +655,12 @@
         start_pair(1)
         start_pair(2)
         gather_relay(tok_full, 0, 0)
-        from_far(0, 0)
+        for c in range(counts[0]):
+            from_far(0, c)
         gather_finish(tok_full, 0, 0)
         norm_rows(tok_full, mix_gain, 0)
-        for w in range(1, MIXER):
-            from_far(w, 0)
+        for w, c in mixer_tiles[counts[0] :]:
+            from_far(w, c)
 
         @pl.when(has_guest)
         def _():
@@ -662,7 +670,8 @@
         inner_pair(0)
         for w in range(3):
             own_copy(w).wait()
-            finish_all(w, 0)
+            for c in range(counts[w]):
+                finish_all(w, c)
             project(w, 0)
         convolve()
         own_copy(3).wait()
@@ -762,10 +771,13 @@
             for c in range(first, first + count):
                 combine(b, c)
 
+        def take(b, first, count):
+            for c in range(first, first + count):
+                finish(DOWN, c, b)
+            produce(b, first, count)
+
         def near_pieces(first, count):
-            for c in range(first, first + count):
-                finish(DOWN, c, near)
-            produce(near, first, count)
+            take(near, first, count)
 
         produce(f, 0, batch)
         near_pieces(0, batch)
@@ -781,6 +793,7 @@
         far_down(1)
         for c in range(3, pieces):
             outer_down(c)
+        take(outer, 0, 1)
         far_down(2)
         drain(groups[:-1])
         for r in range(2):
@@ -794,11 +807,6 @@
                     b = f + toward * (1 + s)
                     pl.when((b >= 0) & (b < n))(lambda: visit(b))
 
-        def take(b, first, count):
-            for c in range(first, first + count):
-                finish(DOWN, c, b)
-            produce(b, first, count)
-
         def settle_range(first, end):
             @pl.loop(first, end)
             def _(i):
@@ -812,13 +820,15 @@
             others(lambda b: combine(b, c))
 
         far_take(0)
+        join(outer, 0, 1)
         far_join(0)
-        take(outer, 0, batch)
+        for c in range(1, batch):
+            take(outer, c, 1)
         for c in range(3, pieces):
             from_far(DOWN, c)
         for c in range(1, batch):
             far_take(c)
-        join(outer, 0, batch)
+            join(outer, c, 1)
         settle_range(0, batch)
         for c in range(1, batch):
             far_join(c)
@@ -829,11 +839,12 @@
             join(outer, c, 1)
             if c == batch:
                 settle_range(batch, pieces)
+            if c + 1 == pieces:
+                for i in range(batch):
+                    settle(outer, i)
             far_take(c)
         if pieces > batch:
             far_join(pieces - 1)
-            for c in range(batch):
-                settle(outer, c)
         for c in range(pieces):
             others(lambda b: settle(b, c))
             if c >= batch or pieces == batch:
@@ -865,6 +876,9 @@
                 down_sent(r, k)
         drain((DOWN,))
 
+    for i in range(seqs):
+        put_out(i).wait()
+
 
 def solution(mesh):
     n, parts, n_tp = mesh.shape["fs"], mesh.shape["grp"], mesh.shape["tp"]
@@ -875,13 +889,15 @@
         weights = (outer, inner, value, mix_out, gate, up, down)
         piece = min(down.shape[1], columns, 128)
         spans = [((0, a.shape[1]),) for a in weights]
+        if outer.shape[1] % 256 == 0:
+            spans[0] = ((0, outer.shape[1] // 2), (outer.shape[1] // 2, outer.shape[1] // 2))
         spans[GATE] = spans[UP] = tiles_of(gate.shape[1])
         spans[DOWN] = tuple((start, piece) for start in range(0, down.shape[1], piece))
         slots = sum(len(tiles) for w, tiles in enumerate(spans) if w != UP)
         groups = len(weights) - 1
         channels, units = outer.shape[1], gate.shape[1]
         y_others = max(parts - 1, 1)
-        per_owner = columns // piece
+        per_owner, packed = columns // piece, -(-seqs // 8) * 8
         dma = pltpu.SemaphoreType.DMA
         scratch = [pltpu.VMEM((n,) + a.shape, BF16) for a in weights[:GATE]]
         scratch += [pltpu.VMEM((2, n) + gate.shape, BF16), pltpu.VMEM((n,) + down.shape, BF16)]
@@ -899,22 +915,23 @@
             pltpu.VMEM((rows, columns), BF16),
             pltpu.VMEM((rows, columns), F32),
             pltpu.VMEM((2 * rows, 128), F32),
-            pltpu.VMEM((2, seqs, 8, length), F32),
-            pltpu.VMEM((2, n_tp, seqs, 8, length), F32),
-            pltpu.VMEM((seqs, 8, length), F32),
+            pltpu.VMEM((2, packed, length), F32),
+            pltpu.VMEM((2, n_tp, packed, length), F32),
+            pltpu.VMEM((packed, length), F32),
+            pltpu.VMEM((rows, columns), BF16),
             pltpu.VMEM((1, width), F32), pltpu.VMEM(taps.shape, F32),
             pltpu.VMEM((1, width), F32), pltpu.VMEM((1, width), F32),
             dma((groups, n + 1)), dma((slots, n - 1)),
             dma((groups, n, y_others)), dma((slots, n - 1, y_others)),
             dma((12,)), dma((3, 2, chips)), dma((3, 2, chips)), dma((3, 2, chips)), dma((3, 2, chips)),
             dma((2, chips)), dma((2, chips, per_owner)), dma((2, chips)), dma((2, chips, per_owner)),
-            dma((2, n_tp)), dma((2, n_tp)), dma((1,)), dma((per_owner,)), dma((2,)),
+            dma((2, n_tp)), dma((2, n_tp)), dma((1,)), dma((per_owner,)), dma((2,)), dma((seqs,)),
         ]
         out = pl.pallas_call(
             functools.partial(kernel, n, parts, n_tp, length, tuple(spans)),
             out_shape=jax.ShapeDtypeStruct((rows, columns), BF16),
             in_specs=[pl.BlockSpec(memory_space=pl.ANY)] * 12,
-            out_specs=pl.BlockSpec(memory_space=pltpu.VMEM),
+            out_specs=pl.BlockSpec(memory_space=pl.ANY),
             scratch_shapes=scratch,
             compiler_params=pltpu.CompilerParams(
                 collective_id=0, has_side_effects=True, vmem_limit_bytes=62 * 1024 * 1024

time: 148 us -> 147 us (level)
  no operation moved by 1% of the time
where the time goes in v4:
time: 147 us
  Pallas kernels  145 us (99%)
  local copies, waits for them, and re-layouts  1.87 us (1%)
    pallas_call x1, Pallas kernels, local(): pl.pallas_call(functools.partial(kernel, n, parts, n_tp, length, tuple(sp...  145 us

profile of v4, /device:TPU:0, one launch (start us, length us, event | category | flops | bytes accessed | tf_op | source)
XLA Modules:
  0.0 147.2 jit_solution(676708677394966896)
XLA Ops:
  0.0 145.3 %shard_map.118 = bf16[512,512]{1,0:T(8,128)(2,1)} custom-call(bf16[512,512]{1,0:T(8,128)(2,1)} %bitcast.6, f32[1,2048]{1,0:T(1,128)} %bitcast.7, bf16[512,256]{1,0:T(8,128)(2,1)} %w0.1, bf16[512,256]{1,0:T(8,128)(2,1)} %w1.1, bf16[512,256]{1,0:T(8,128)(2,1)} %w2.1, f32[3,1024]{1,0:T(4,128)} %taps_in.1, bf16[256,512]{1,0:T(8,128)(2,1)} %w3.1, ...), custom_call_target="tpu_custom_call" | custom-call | tf_op jit(solution)/shard_map/pallas_call | solution.py:930
  145.3 1.9 %copy.14 = bf16[4,128,512]{2,1,0:T(8,128)(2,1)} copy(bf16[4,128,512]{2,1,0:T(8,128)(2,1)} %bitcast.5) | data formatting | bytes 1048576

commit v5 on v4

--- a/solution.py
+++ b/solution.py
@@ -12,7 +12,7 @@
 BF16 = jnp.bfloat16
 MIXER = 4
 GATE, UP, DOWN = 4, 5, 6
-SHARED = 1
+SHARED = 2
 TRAIL = 2
 LAG = 2
 

time: 147 us -> 147 us (level)
  no operation moved by 1% of the time
where the time goes in v5:
time: 147 us
  Pallas kernels  145 us (99%)
  local copies, waits for them, and re-layouts  1.87 us (1%)
    pallas_call x1, Pallas kernels, local(): pl.pallas_call(functools.partial(kernel, n, parts, n_tp, length, tuple(sp...  145 us

profile of v5, /device:TPU:0, one launch (start us, length us, event | category | flops | bytes accessed | tf_op | source)
XLA Modules:
  0.0 146.8 jit_solution(6377496489198720534)
XLA Ops:
  0.0 145.0 %shard_map.118 = bf16[512,512]{1,0:T(8,128)(2,1)} custom-call(bf16[512,512]{1,0:T(8,128)(2,1)} %bitcast.6, f32[1,2048]{1,0:T(1,128)} %bitcast.7, bf16[512,256]{1,0:T(8,128)(2,1)} %w0.1, bf16[512,256]{1,0:T(8,128)(2,1)} %w1.1, bf16[512,256]{1,0:T(8,128)(2,1)} %w2.1, f32[3,1024]{1,0:T(4,128)} %taps_in.1, bf16[256,512]{1,0:T(8,128)(2,1)} %w3.1, ...), custom_call_target="tpu_custom_call" | custom-call | tf_op jit(solution)/shard_map/pallas_call | solution.py:930
  145.0 1.9 %copy.14 = bf16[4,128,512]{2,1,0:T(8,128)(2,1)} copy(bf16[4,128,512]{2,1,0:T(8,128)(2,1)} %bitcast.5) | data formatting | bytes 1048576
